TPU v7x, 128 devices: a whole 4x4x4 slice. The times are simulated.
128 devices in a mesh: sp: 32 (over z, y, core), tp: 4 (over x).
Axes of the slice: x: 4, y: 4, z: 4, core: 2. Of those that a mesh axis runs over, the one named last changes fastest.
Arguments:
- tokens: bfloat16 [32768, 4096], P('sp', 'tp'), may hold values from -16 to 16
- norm_gain: float32 [4096], replicated, may hold values from 0.1 to 1.9
- w_pool_in: bfloat16 [4096, 2048], P('sp', 'tp'), may hold values from -0.09375 to 0.09375
- w_query: bfloat16 [4096, 2048], P('sp', 'tp'), may hold values from -0.09375 to 0.09375
- w_key: bfloat16 [4096, 256], P('sp', 'tp'), may hold values from -0.09375 to 0.09375
- w_value: bfloat16 [4096, 256], P('sp', 'tp'), may hold values from -0.09375 to 0.09375
- pool_map: bfloat16 [4, 512, 512], P('tp'), may hold values from -0.25 to 0.25
- pool_scale: float32 [2048], P('tp'), may hold values from 0.3 to 3
- q_gain: float32 [64], replicated, may hold values from 0.1 to 1.9
- k_gain: float32 [64], replicated, may hold values from 0.1 to 1.9
- sinks: float32 [32], P('tp'), may hold values from 0 to 4
- w_out: bfloat16 [4096, 4096], P('tp', 'sp'), may hold values from -0.09375 to 0.09375
Outputs:
- layer_out: bfloat16 [32768, 4096], P(('sp', 'tp'))
All inputs are finite; a program needn't handle non-finite values.
Results may differ from a plain program's by a relative error of at most 0.012.
Values may be sent and summed in bfloat16 or wider, within the bound.
A program may use at most 128 MiB of HBM per device.

v0:
```python
import jax
import jax.numpy as jnp
from jax import lax
from jax.sharding import PartitionSpec as P

HEAD_DIM = 64
GROUP = 8
WINDOW = 128
GROUP_WIDTH = 512
Q_HEADS = 32


epsilon = 1e-06


def copy_for_each(x, axis):
    copies = jnp.broadcast_to(x, (lax.axis_size(axis), *x.shape))
    return lax.all_to_all(copies, axis, split_axis=0, concat_axis=0, tiled=True)


def joined_along(tiles, dim):
    tiles = jnp.moveaxis(tiles, 0, dim)
    dims = tiles.shape
    return tiles.reshape(*dims[:dim], dims[dim] * dims[dim + 1], *dims[dim + 2 :])


def collect(x, axis, dim):
    tiles = copy_for_each(x, axis)
    return joined_along(tiles, dim)


def sent_together(arrays, axis, dim, along):
    widths = [a.shape[along] for a in arrays]
    both = jnp.concatenate(arrays, axis=along)
    whole = lax.all_gather(both, axis, axis=dim, tiled=True)
    return tuple(jnp.split(whole, [sum(widths[:k]) for k in range(1, len(widths))], axis=along))


def passed_along(value, axis, steps):
    count = lax.axis_size(axis)
    first, last = (max(0, -steps), min(count, count - steps))
    return lax.ppermute(value, axis, [(source, source + steps) for source in range(first, last)])


def rms_scale(values):
    return values * lax.rsqrt(jnp.mean(values * values, axis=-1, keepdims=True) + epsilon)


def local(
    tokens,
    norm_gain,
    w_pool_in,
    w_query,
    w_key,
    w_value,
    pool_map,
    pool_scale,
    q_gain,
    k_gain,
    sinks,
    w_out,
):
    tok_rows = tokens.shape[0]
    local_groups = w_key.shape[1] // HEAD_DIM
    seq_index = lax.axis_index("sp")
    group_first = lax.axis_index("tp") * local_groups
    gathered = collect(tokens, "tp", 1)
    widened = gathered.astype(jnp.float32)
    normed = (rms_scale(widened) * norm_gain).astype(jnp.bfloat16)
    ext_rows = normed.shape[0]
    pieces = sent_together((w_pool_in, w_query, w_key, w_value), "sp", 0, 1)
    pool_sum, query_sum, key_sum, value_sum = tuple(
        (
            jnp.dot(normed, weight_piece, preferred_element_type=jnp.float32)
            for weight_piece in pieces
        )
    )
    pool_in = pool_sum.astype(jnp.bfloat16)
    query_rows = lax.optimization_barrier(query_sum.astype(jnp.bfloat16))
    key_rows = lax.optimization_barrier(key_sum.astype(jnp.bfloat16))
    value_rows = value_sum.astype(jnp.bfloat16).reshape(ext_rows, local_groups, HEAD_DIM)
    query_float = query_rows.astype(jnp.float32).reshape(ext_rows, local_groups * GROUP, HEAD_DIM)
    query_normed = (
        (rms_scale(query_float) * q_gain)
        .astype(jnp.bfloat16)
        .reshape(ext_rows, local_groups, GROUP, HEAD_DIM)
    )
    key_float = key_rows.astype(jnp.float32).reshape(ext_rows, local_groups, HEAD_DIM)
    key_normed = (rms_scale(key_float) * k_gain).astype(jnp.bfloat16)
    key_width = local_groups * HEAD_DIM
    pair_tail = jnp.concatenate(
        [
            key_normed[tok_rows - WINDOW :].reshape(WINDOW, key_width),
            value_rows[tok_rows - WINDOW :].reshape(WINDOW, key_width),
        ],
        axis=1,
    )
    earlier_pairs, earlier_pool = passed_along((pair_tail, pool_in[tok_rows - 15 :]), "sp", 1)
    key_span = jnp.concatenate(
        [earlier_pairs[:, :key_width].reshape(WINDOW, local_groups, HEAD_DIM), key_normed], axis=0
    )
    value_span = jnp.concatenate(
        [earlier_pairs[:, key_width:].reshape(WINDOW, local_groups, HEAD_DIM), value_rows], axis=0
    )
    pool_span = jnp.concatenate([earlier_pool, pool_in], axis=0)
    positions = seq_index * tok_rows + jnp.arange(tok_rows, dtype=jnp.int32)
    group_ids = group_first + jnp.arange(local_groups, dtype=jnp.int32)
    spans = jnp.exp2((group_ids + 1).astype(jnp.float32))
    pool_float = pool_span.astype(jnp.float32).reshape(tok_rows + 15, local_groups, GROUP_WIDTH)
    sum_two = pool_float[1:] + pool_float[:-1]
    sum_four = sum_two[2:] + sum_two[:-2]
    sum_eight = sum_four[4:] + sum_four[:-4]
    sum_sixteen = sum_eight[8:] + sum_eight[:-8]
    span_pick = spans[None, :, None]
    running = jnp.where(
        span_pick < 3.0,
        sum_two[14 : 14 + tok_rows],
        jnp.where(
            span_pick < 6.0,
            sum_four[12 : 12 + tok_rows],
            jnp.where(span_pick < 12.0, sum_eight[8 : 8 + tok_rows], sum_sixteen),
        ),
    )
    counts = jnp.minimum(positions.astype(jnp.float32)[:, None] + 1.0, spans[None, :])
    pool_diff = (running / counts[:, :, None] - pool_float[15:]).astype(jnp.bfloat16)
    mapped = jnp.einsum("tlc,lcd->tld", pool_diff, pool_map, preferred_element_type=jnp.float32)
    pool_branch = rms_scale(mapped * pool_scale.reshape(local_groups, GROUP_WIDTH))
    blocks = tok_rows // WINDOW
    query_blocks = query_normed.reshape(blocks, WINDOW, local_groups, GROUP, HEAD_DIM)
    key_pairs = jnp.concatenate(
        [
            key_span[:tok_rows].reshape(blocks, WINDOW, local_groups, HEAD_DIM),
            key_span[WINDOW:].reshape(blocks, WINDOW, local_groups, HEAD_DIM),
        ],
        axis=1,
    )
    value_pairs = jnp.concatenate(
        [
            value_span[:tok_rows].reshape(blocks, WINDOW, local_groups, HEAD_DIM),
            value_span[WINDOW:].reshape(blocks, WINDOW, local_groups, HEAD_DIM),
        ],
        axis=1,
    )
    scores = jnp.einsum(
        "nqlgd,nkld->nlgqk", query_blocks, key_pairs, preferred_element_type=jnp.float32
    ) * HEAD_DIM ** (-0.5)
    query_pos = jnp.arange(WINDOW, dtype=jnp.int32)[:, None] + WINDOW
    key_pos = jnp.arange(2 * WINDOW, dtype=jnp.int32)[None, :]
    distance = query_pos - key_pos
    in_band = (distance >= 0) & (distance < WINDOW)
    key_global = (
        seq_index * tok_rows
        + jnp.arange(blocks, dtype=jnp.int32)[:, None] * WINDOW
        - WINDOW
        + jnp.arange(2 * WINDOW, dtype=jnp.int32)[None, :]
    )
    allowed = in_band[None] & (key_global >= 0)[:, None, :]
    head_ids = group_ids[:, None] * GROUP + jnp.arange(GROUP, dtype=jnp.int32)[None, :] + 1
    slopes = jnp.exp2(-8.0 * head_ids.astype(jnp.float32) / Q_HEADS)
    logits = (
        scores - slopes[None, :, :, None, None] * distance.astype(jnp.float32)[None, None, None]
    )
    exp_scores = jnp.exp(jnp.where(allowed[:, None, None], logits, -jnp.inf))
    sink_logits = sinks.reshape(local_groups, GROUP)
    denominator = jnp.sum(exp_scores, axis=-1) + jnp.exp(sink_logits)[None, :, :, None]
    weights_bf = (exp_scores / denominator[..., None]).astype(jnp.bfloat16)
    attended = jnp.einsum(
        "nlgqk,nkld->nqlgd", weights_bf, value_pairs, preferred_element_type=jnp.float32
    )
    attn_branch = rms_scale(attended.reshape(tok_rows, local_groups, GROUP_WIDTH))
    mixed_rows = (
        jnp.stack([pool_branch, attn_branch], axis=2)
        .reshape(tok_rows, 2 * local_groups * GROUP_WIDTH)
        .astype(jnp.bfloat16)
    )
    out_columns = lax.all_gather(w_out, "sp", axis=1, tiled=True)
    return lax.psum_scatter(
        jnp.dot(mixed_rows, out_columns, preferred_element_type=jnp.float32).astype(jnp.bfloat16),
        "tp",
        scatter_dimension=0,
        tiled=True,
    )


def solution(mesh):
    in_specs = (
        P("sp", "tp"),
        P(),
        P("sp", "tp"),
        P("sp", "tp"),
        P("sp", "tp"),
        P("sp", "tp"),
        P("tp", None, None),
        P("tp"),
        P(),
        P(),
        P("tp"),
        P("tp", "sp"),
    )
    out_specs = P(("sp", "tp"), None)
    return jax.shard_map(local, mesh=mesh, in_specs=in_specs, out_specs=out_specs, check_vma=False)
```

profile of v0, /device:TPU:1, one launch (start us, length us, event | category | flops | bytes accessed | tf_op | source)
XLA Modules:
  0.0 283.9 jit_solution(12096752414852724461)
XLA Ops:
  6.5 0.9 copy.23
  7.4 0.8 copy.24
  8.3 1.8 concatenate.21
  10.1 2.9 %copy.22 = bf16[1024,1024]{0,1:T(8,128)(2,1)S(1)} copy(bf16[1024,1024]{1,0:T(8,128)(2,1)} %param.12) | data formatting | bytes 4194304 | tf_op args[0]
  12.9 4.4 %broadcast_in_dim.65 = bf16[4,1024,1024]{1,2,0:T(8,128)(2,1)} broadcast(bf16[1024,1024]{0,1:T(8,128)(2,1)S(1)} %copy.22), dimensions={1,2} | broadcast | bytes 10485760 | tf_op jit(solution)/shard_map/broadcast_in_dim | solution.py:17
  17.3 5.8 %all-to-all-start = ((bf16[4,1024,1024]{1,2,0:T(8,128)(2,1)}), bf16[4,1024,1024]{1,2,0:T(8,128)(2,1)}, u32[]{:S(2)}, u32[]{:S(2)}) async-start(bf16[4,1024,1024]{1,2,0:T(8,128)(2,1)} %broadcast_in_dim.65), calls=%async_computation | async-start | bytes 16777216 | tf_op jit(solution)/shard_map/all_to_all | solution.py:18
  23.1 0.0 all-gather.5.cloned.1.call-start
  23.1 0.7 all-gather.5.cloned.1.call-update
  23.9 0.1 add_compare_fusion
  24.1 0.3 broadcast_and_fusion
  24.5 1.2 broadcast_multiply_fusion
  25.6 91.2 %all-to-all-done = bf16[4,1024,1024]{1,2,0:T(8,128)(2,1)} async-done(((bf16[4,1024,1024]{1,2,0:T(8,128)(2,1)}), bf16[4,1024,1024]{1,2,0:T(8,128)(2,1)}, u32[]{:S(2)}, u32[]{:S(2)}) %all-to-all-start) | async-done | bytes 8388640 | tf_op jit(solution)/shard_map/all_to_all | solution.py:18
  116.8 5.4 %multiply_reduce_fusion = f32[1024]{0:T(1024)S(1)} fusion(bf16[4,1024,1024]{1,2,0:T(8,128)(2,1)} %all-to-all-done), kind=kLoop, calls=%fused_computation.3 | loop fusion | flops 12581888 | bytes 8392704 | tf_op jit(solution)/shard_map/reduce_sum | solution.py:46
  122.2 7.8 %fusion.1 = bf16[1024,4096]{0,1:T(8,128)(2,1)} fusion(f32[4096]{0:T(1024)S(1)} %copy-done.7, f32[1024]{0:T(1024)S(1)} %add_rsqrt_fusion.2, bf16[4,1024,1024]{1,2,0:T(8,128)(2,1)} %all-to-all-done), kind=kLoop, calls=%fused_computation.2 | loop fusion | flops 16777216 | bytes 16797696 | tf_op jit(solution)/shard_map/convert_element_type | solution.py:69
  130.0 9.2 %fusion.19 = bf16[1024,512]{1,0:T(8,128)(2,1)S(1)} fusion(bf16[1024,4096]{0,1:T(8,128)(2,1)} %fusion.1, bf16[4096,1152]{1,0:T(8,128)(2,1)} %all-gather.3.cloned.1.call-done), kind=kOutput, calls=%fused_computation.34 | convolution fusion | flops 4295491584 | bytes 13631488 | tf_op jit(solution)/shard_map/dot_general | solution.py:74
  139.3 5.3 %collective-permute-start = (bf16[15,512]{1,0:T(8,128)(2,1)S(1)}, bf16[15,512]{1,0:T(8,128)(2,1)S(1)}, u32[]{:S(2)}, u32[]{:S(2)}) collective-permute-start(bf16[15,512]{1,0:T(8,128)(2,1)S(1)} %slice.86), channel_id=1, source_target_pairs={{0,4},{4,8},{8,12},{12,16},{16,20},{20,24},{24,28},{28,32},{32,36}... | collective-permute-start | bytes 46088 | tf_op jit(solution)/shard_map/ppermute | solution.py:42
  144.6 1.6 convolution_convert_fusion.2
  146.3 0.1 fusion.35
  146.4 2.0 convolution_convert_fusion.1
  148.4 2.1 collective-permute-start.1
  150.5 5.5 %fusion.22 = bf16[1024,512]{1,0:T(8,128)(2,1)} fusion(bf16[1024,4096]{0,1:T(8,128)(2,1)S(1)} %copy-done.2, bf16[4096,1152]{1,0:T(8,128)(2,1)S(1)} %copy-done.11), kind=kOutput, calls=%fused_computation.35 | convolution fusion | flops 4295491584 | bytes 13631488 | tf_op jit(solution)/shard_map/dot_general | solution.py:74
  156.0 1.5 copy.29
  157.5 2.8 convert_multiply_fusion
  160.3 2.9 %copy.30 = f32[1024,512]{0,1:T(8,128)} copy(f32[1024,512]{1,0:T(8,128)} %convert_multiply_fusion) | data formatting | bytes 4194304 | tf_op jit(solution)/shard_map/mul | solution.py:46
  163.3 1.8 bitcast_reduce_fusion
  165.2 0.5 copy.42
  165.6 0.1 fusion.56
  165.7 0.1 copy-done.10
  165.8 0.3 multiply_convert_fusion.1
  166.1 0.1 fusion.57
  166.3 0.7 copy-done.5
  167.0 0.3 maximum_convert_fusion
  167.3 0.3 slice_add_fusion.1
  167.6 0.3 slice_add_fusion
  167.9 0.3 slice_add_fusion.2
  168.2 0.4 copy-done.9
  168.6 1.4 multiply_reduce_fusion.2
  170.0 1.2 fusion.25
  171.4 2.5 fusion.4
  173.9 0.1 broadcast_add_fusion
  173.9 2.4 multiply_reduce_fusion.1
  176.4 2.5 copy.34
  178.9 1.7 reshape.366
  180.6 0.3 multiply_convert_fusion
  180.9 0.9 copy-done.3
  181.8 0.2 pad_maximum_fusion
  182.1 14.8 %convolution_convert_fusion = bf16[1024,4096]{1,0:T(8,128)(2,1)} fusion(bf16[1024,1024]{0,1:T(8,128)(2,1)S(1)} %bitcast.125, bf16[1024,4096]{1,0:T(8,128)(2,1)} %all-gather.5.cloned.1.call-done), kind=kOutput, calls=%fused_computation.8 | convolution fusion | flops 8594128896 | bytes 18874368 | tf_op jit(solution)/shard_map/dot_general | solution.py:178
  196.9 80.5 %reduce-scatter.2.cloned.1.call-done = bf16[256,4096]{1,0:T(8,128)(2,1)} async-done(((bf16[1024,4096]{1,0:T(8,128)(2,1)}), bf16[256,4096]{1,0:T(8,128)(2,1)}) %reduce-scatter.2.cloned.1.call-update) | async-done | bytes 2097168 | tf_op jit(solution)/shard_map/reduce_scatter | solution.py:177
  (56 shorter events, 0.5 us)
Async XLA Ops:
  6.5 161.7 %copy-start = (bf16[1,512,512]{2,1,0:T(8,128)(2,1)S(1)}, bf16[1,512,512]{2,1,0:T(8,128)(2,1)}, u32[]{:S(2)}) copy-start(bf16[1,512,512]{2,1,0:T(8,128)(2,1)} %param.18) | copy-start | bytes 1572868
  6.5 123.4 %all-gather.3.cloned.1.call-start = ((), (), s32[]{:S(2)}) async-start(), calls=%async_computation.2 | async-start | bytes 9732096 | tf_op jit(solution)/shard_map/all_gather | solution.py:35
  17.3 6.7 %copy-start.12 = (f32[8]{0:T(128)S(1)}, f32[8]{0:T(128)}, u32[]{:S(2)}) copy-start(f32[8]{0:T(128)} %param.22) | copy-start | bytes 100
  17.3 99.5 %all-to-all-start = ((bf16[4,1024,1024]{1,2,0:T(8,128)(2,1)}), bf16[4,1024,1024]{1,2,0:T(8,128)(2,1)}, u32[]{:S(2)}, u32[]{:S(2)}) async-start(bf16[4,1024,1024]{1,2,0:T(8,128)(2,1)} %broadcast_in_dim.65), calls=%async_computation | async-start | bytes 16777216 | tf_op jit(solution)/shard_map/all_to_all | solution.py:18
  23.1 159.0 %all-gather.5.cloned.1.call-start = ((), (), s32[]{:S(2)}) async-start(), calls=%async_computation.3 | async-start | bytes 8650752 | tf_op jit(solution)/shard_map/all_gather | solution.py:176
  23.8 253.6 %reduce-scatter.2.cloned.1.call-start = ((), (), s32[]{:S(2)}) async-start(), calls=%async_computation.4 | async-start | bytes 10485760 | tf_op jit(solution)/shard_map/reduce_scatter | solution.py:177
  25.6 96.5 %copy-start.7 = (f32[4096]{0:T(1024)S(1)}, f32[4096]{0:T(1024)}, u32[]{:S(2)}) copy-start(f32[4096]{0:T(1024)} %param.13) | copy-start | bytes 49156
  130.0 14.6 %copy-start.2 = (bf16[1024,4096]{0,1:T(8,128)(2,1)S(1)}, bf16[1024,4096]{0,1:T(8,128)(2,1)}, u32[]{:S(2)}) copy-start(bf16[1024,4096]{0,1:T(8,128)(2,1)} %fusion.1) | copy-start | bytes 25165828
  130.0 14.6 %copy-start.11 = (bf16[4096,1152]{1,0:T(8,128)(2,1)S(1)}, bf16[4096,1152]{1,0:T(8,128)(2,1)}, u32[]{:S(2)}) copy-start(bf16[4096,1152]{1,0:T(8,128)(2,1)} %all-gather.3.cloned.1.call-done) | copy-start | bytes 28311556
  139.2 7.0 %copy-start.4 = (bf16[1024,512]{1,0:T(8,128)(2,1)}, bf16[1024,512]{1,0:T(8,128)(2,1)S(1)}, u32[]{:S(2)}) copy-start(bf16[1024,512]{1,0:T(8,128)(2,1)S(1)} %fusion.19) | copy-start | bytes 3145732
  139.2 7.1 %copy-start.8 = (f32[64]{0:T(128)S(1)}, f32[64]{0:T(128)}, u32[]{:S(2)}) copy-start(f32[64]{0:T(128)} %param.21) | copy-start | bytes 772
  139.3 27.0 %collective-permute-start = (bf16[15,512]{1,0:T(8,128)(2,1)S(1)}, bf16[15,512]{1,0:T(8,128)(2,1)S(1)}, u32[]{:S(2)}, u32[]{:S(2)}) collective-permute-start(bf16[15,512]{1,0:T(8,128)(2,1)S(1)} %slice.86), channel_id=1, source_target_pairs={{0,4},{4,8},{8,12},{12,16},{16,20},{20,24},{24,28},{28,32},{32,36}... | collective-permute-start | bytes 46088 | tf_op jit(solution)/shard_map/ppermute | solution.py:42
  148.4 22.8 %collective-permute-start.1 = (bf16[128,128]{0,1:T(8,128)(2,1)S(1)}, bf16[128,128]{0,1:T(8,128)(2,1)S(1)}, u32[]{:S(2)}, u32[]{:S(2)}) collective-permute-start(bf16[128,128]{0,1:T(8,128)(2,1)S(1)} %pad_maximum_fusion.3), channel_id=1, source_target_pairs={{0,4},{4,8},{8,12},{12,16},{16,20},{20,24},{24,28},{28,32},{32,36}... | collective-permute-start | bytes 98312 | tf_op jit(solution)/shard_map/ppermute | solution.py:42
  165.1 0.7 copy-start.10
  165.8 1.2 copy-start.5
  167.9 0.7 copy-start.9
  170.0 1.3 copy-start.6
  180.6 1.2 copy-start.3
  196.8 80.5 %copy-start.1 = (bf16[1,512,512]{2,1,0:T(8,128)(2,1)S(1)}, bf16[1,512,512]{2,1,0:T(8,128)(2,1)}, u32[]{:S(2)}) copy-start(bf16[1,512,512]{2,1,0:T(8,128)(2,1)} %param.18) | copy-start | bytes 1572868
Sparse Core Ops, SparseCore 0:
  10.2 58.9 all-gather.2
  71.3 58.4 all-gather.4
  197.0 80.3 reduce-scatter.1
where the time goes:
time: 285 us; the launch traced here: 284 us
  waiting for transfers between devices  172 us (60%)
  matrix products  39.4 us (14%)
  other arithmetic  23 us (8%)
  local copies, waits for them, and re-layouts  22.2 us (8%)
  between operations  13.6 us (5%)
  starting transfers between devices  13.3 us (5%)
    all_to_all x1, waiting for transfers between devices, copy_for_each(): return lax.all_to_all(copies, axis, split_axis=0, concat_axis=0, tiled=True)  91.2 us
    reduce_scatter x1, waiting for transfers between devices, local(): lax.psum_scatter(jnp.dot(mixed_rows, out_columns, preferred_element_type=...  80.5 us
    dot_general x4, matrix products, local(): jnp.dot(normed, weight_piece, preferred_element_type=jnp.float32)  18.3 us
    dot_general x1, matrix products, local(): jnp.dot(mixed_rows, out_columns, preferred_element_type=jnp.float32)  14.8 us
    convert_element_type x1, other arithmetic, local(): normed = (rms_scale(widened) * norm_gain).astype(jnp.bfloat16)  7.79 us
    ppermute x2, starting transfers between devices, passed_along(): lax.ppermute(value, axis, [(source, source + steps) for source in range(f...  7.42 us
    unnamed x32, local copies, waits for them, and re-layouts  7.27 us
    reduce_sum x3, other arithmetic, rms_scale(): jnp.mean(values * values, axis=-1, keepdims=True) + epsilon  7.22 us
  transfers between devices with their start and end apart: 6, of which 2 were waited for; matrix products, arithmetic and copies ran while one was open for 23% of the time, Pallas kernels for 0%

commit v1 on v0

v1 whole, which is shorter than its diff:
```python
import jax
import jax.numpy as jnp
from jax import lax
from jax.experimental import pallas as pl
from jax.experimental.pallas import tpu as pltpu
from jax.sharding import PartitionSpec as P

MESH = pl.DeviceIdType.MESH
F32 = jnp.float32
BF16 = jnp.bfloat16
EPS = 1e-6
N_COPIES = 96


def mod4(v):
    return lax.rem(v, 4)


def kernel(
    tokens, wp, wq, wkv, wo, pmap, prm_in, gain,
    own_out, recv_out,
    W1, W2, TOK, ST1, ST2, ST3, PM, PRM, KV, PB, QB, ACC, SS, MIX, BIAS, BLK, SENDB, OWNB,
    lsem, ssem, rsem, osend, orecv, oloc, hsend, hrecv,
):
    sp = lax.axis_index("sp")
    x = lax.axis_index("tp")
    c = lax.rem(sp, 2)
    y = mod4(lax.div(sp, 2))
    z = lax.div(sp, 8)
    f = y + c * (z - y)
    s = z + c * (y - z)
    par = lax.rem(x, 2)
    flip1 = x + 1 - 2 * par
    flip3 = 3 - x
    p = (1 - c) * flip1 + c * flip3
    n = (1 - c) * flip3 + c * flip1
    x2 = mod4(x + 2)
    dx = mod4(x + 1 + 2 * c)

    def sp_of(c_, f_, s_):
        y_ = (1 - c_) * f_ + c_ * s_
        z_ = (1 - c_) * s_ + c_ * f_
        return (z_ * 4 + y_) * 2 + c_

    fu, fd = mod4(f + 1), mod4(f + 3)
    su, sd, s2 = mod4(s + 1), mod4(s + 3), mod4(s + 2)
    dev_fu, dev_fd = (sp_of(c, fu, s), x), (sp_of(c, fd, s), x)
    dev_su, dev_sd = (sp_of(c, f, su), x), (sp_of(c, f, sd), x)
    dev_sib = (sp + 1 - 2 * c, x)
    dev_dx, dev_p, dev_n, dev_x2 = (sp, dx), (sp, p), (sp, n), (sp, x2)
    cs, ss_, sf_ = 1 - c, f, s
    ssu, ssd, ss2 = mod4(ss_ + 1), mod4(ss_ + 3), mod4(ss_ + 2)

    pending = []

    def send(src, dst, dev):
        k = len(pending)
        d = pltpu.make_async_remote_copy(
            src_ref=src, dst_ref=dst, send_sem=ssem.at[k], recv_sem=rsem.at[k],
            device_id=dev, device_id_type=MESH,
        )
        d.start()
        pending.append(d)
        return d

    def recv(*ds):
        for d in ds:
            d.wait_recv()

    loc = []

    def local(src, dst):
        d = pltpu.make_async_copy(src, dst, lsem.at[len(loc)])
        d.start()
        loc.append(d)
        return d

    own1 = W1.at[0, c, s, f]
    l0 = local(wp, own1.at[:, pl.ds(0, 512)])
    l1 = local(wq, own1.at[:, pl.ds(512, 512)])
    l2 = local(wkv, own1.at[:, pl.ds(1024, 128)])
    l3 = local(wo, W2.at[c, s, f, 0])
    l4 = local(tokens.at[pl.ds(x * 256, 256)], TOK.at[0, x])
    l5 = local(tokens.at[pl.ds(p * 256, 256)], TOK.at[1, x])
    l6 = local(pmap, PM.at[0])
    l7 = local(prm_in, PRM.at[0])

    l0.wait()
    l1.wait()
    l2.wait()
    x_w1 = send(own1, ST1, dev_dx)
    a1 = [send(own1, own1, dev_fu), send(own1, own1, dev_fd)]
    tn = [
        send(tokens.at[pl.ds(n * 256, 256)], TOK.at[0, x], dev_n),
        send(tokens.at[pl.ds(x2 * 256, 256)], TOK.at[1, x], dev_n),
    ]
    tp_ = [
        send(tokens.at[pl.ds(p * 256, 256)], TOK.at[0, x], dev_p),
        send(tokens.at[pl.ds(x * 256, 256)], TOK.at[1, x], dev_p),
    ]
    prm_c = send(prm_in, PRM.at[1], dev_x2)
    l3.wait()
    x_w2 = send(W2.at[c, s, f, 0], ST2, dev_dx)
    l6.wait()
    half = pl.ds(c * 256, 256)
    x_pm = send(PM.at[0, half], ST3, dev_dx)

    lane_i = lax.broadcasted_iota(jnp.int32, (512, 512), 1)
    row_i = lax.broadcasted_iota(jnp.int32, (512, 512), 0)
    BLK[...] = jnp.where(
        lax.shift_right_logical(lane_i, 6) == lax.shift_right_logical(row_i, 6), 1.0, 0.0
    ).astype(BF16)
    SS[...] = jnp.zeros_like(SS)

    recv(x_w1)
    f_w1 = send(ST1, W1.at[1, c, s, f], dev_dx)

    def step_b1(g, a):
        recv(*a)
        return [
            send(W1.at[g, c, s, fd, pl.ds(0, 64)], W1.at[g, c, s, fd, pl.ds(0, 64)], dev_fu),
            send(W1.at[g, c, s, fu, pl.ds(64, 64)], W1.at[g, c, s, fu, pl.ds(64, 64)], dev_fd),
        ]

    def step_c1(g, b):
        recv(*b)
        plane = W1.at[g, c, s]
        return [send(plane, plane, dev_su), send(plane, plane, dev_sd)], [send(plane, plane, dev_sib)]

    def step_d1(g, cc, sib):
        recv(*cc)
        lo, hi = W1.at[g, c, sd], W1.at[g, c, su]
        d = [
            send(lo.at[pl.ds(0, 2)], lo.at[pl.ds(0, 2)], dev_su),
            send(hi.at[pl.ds(2, 2)], hi.at[pl.ds(2, 2)], dev_sd),
        ]
        sib += [send(lo, lo, dev_sib), send(hi, hi, dev_sib)]
        return d

    def step_e1(g, d, sib):
        recv(*d)
        far = W1.at[g, c, s2]
        sib.append(send(far, far, dev_sib))

    b1 = step_b1(0, a1)
    c1, sib1 = step_c1(0, b1)
    recv(f_w1)
    oth1 = W1.at[1, c, s, f]
    a1o = [send(oth1, oth1, dev_fu), send(oth1, oth1, dev_fd)]

    def scale_slab(j):
        g = gain[:, pl.ds(pl.multiple_of(j * 1024, 1024), 1024)]

        def body(k, carry):
            slot, r = lax.div(k, 4), pl.ds(lax.rem(k, 4) * 64, 64)
            t = TOK[slot, j, r, :].astype(F32)
            sq = t * t
            tot = sq[:, 0:128]
            for m in range(1, 8):
                tot += sq[:, m * 128 : (m + 1) * 128]
            SS[slot, r, :] += tot
            TOK[slot, j, r, :] = (t * g).astype(BF16)
            return carry

        lax.fori_loop(0, 8, body, 0)

    l4.wait()
    l5.wait()
    scale_slab(x)

    recv(*tn)
    tf = [
        send(TOK.at[0, n], TOK.at[1, n], dev_p),
        send(TOK.at[1, n], TOK.at[0, n], dev_p),
    ]
    b1o = step_b1(1, a1o)
    recv(x_w2)
    f_w2 = send(ST2, W2.at[c, s, f, 1], dev_dx)
    recv(x_pm)
    f_pm = send(ST3, PM.at[1, half], dev_dx)
    c1o, sib1o = step_c1(1, b1o)
    recv(f_w2)
    own2 = W2.at[c, s, f]
    a2 = [send(own2, own2, dev_fu), send(own2, own2, dev_fd)]

    recv(*tp_)
    scale_slab(p)

    l7.wait()
    recv(prm_c)
    key_i = jnp.bitwise_and(lane_i, 255)
    dist = 128 + jnp.bitwise_and(row_i, 127) - key_i
    band = (dist >= 0) & (dist < 128)
    head_in = 2 * lax.shift_right_logical(row_i, 7) + lax.shift_right_logical(lane_i, 8) + 1
    for gi, g in ((0, x), (1, x2)):
        slope = jnp.exp2(-0.25 * (g * 8 + head_in).astype(F32))
        BIAS[gi] = jnp.where(band, -slope * dist.astype(F32), -1e30)

    d1 = step_d1(0, c1, sib1)
    recv(*a2)
    b2 = [
        send(W2.at[c, s, fd, 0], W2.at[c, s, fd, 0], dev_fu),
        send(W2.at[c, s, fu, 1], W2.at[c, s, fu, 1], dev_fd),
    ]
    recv(f_pm)
    sib_pm = send(PM.at[1, half], PM.at[1, half], dev_sib)
    for d in tf:
        d.wait_send()
    scale_slab(n)
    recv(*b2)
    d1o = step_d1(1, c1o, sib1o)

    def half_plane(s_, k):
        return W2.at[c, s_, pl.ds(2 * k, 2)]

    def c2_send(k_up, k_dn):
        u, d = half_plane(s, k_up), half_plane(s, k_dn)
        return [send(u, u, dev_su), send(d, d, dev_sd)]

    c2a = c2_send(0, 1)
    c2b = c2_send(1, 0)
    plane2 = W2.at[c, s]
    sib2_own = [send(plane2, plane2, dev_sib)]

    def matmul(gi, jz):
        parts = []
        for yy in range(4):
            parts.append(W1[gi, 0, jz, yy])
            parts.append(W1[gi, 1, yy, jz])
        rhs = jnp.concatenate(parts, axis=0)
        lhs = TOK[:, jz].reshape(512, 1024)
        ACC[...] += jnp.dot(lhs, rhs, preferred_element_type=F32)

    def matmuls(gi, order):
        ACC[...] = jnp.zeros_like(ACC)

        def body(t, carry):
            matmul(gi, order(t))
            return carry

        return body

    def post(gi):
        def body(k, carry):
            slot, r = lax.div(k, 2), lax.rem(k, 2)
            rows = pl.ds(pl.multiple_of(k * 128, 128), 128)
            tot = jnp.sum(SS[slot, pl.ds(r * 128, 128), :], axis=-1, keepdims=True)
            a = ACC[rows, :] * lax.rsqrt(tot * (1.0 / 4096) + EPS)
            PB[gi, slot, pl.ds(pl.multiple_of(16 + r * 128, 16), 128), :] = a[:, 0:512].astype(BF16)
            qf = a[:, 512:1024].astype(BF16).astype(F32)
            sq = qf * qf
            hi = sq.astype(BF16)
            lo = (sq - hi.astype(F32)).astype(BF16)
            ssq = jnp.dot(hi, BLK[...], preferred_element_type=F32) + jnp.dot(
                lo, BLK[...], preferred_element_type=F32
            )
            qg = jnp.concatenate([PRM[0, 8 + j : 9 + j, :] for j in range(4)], axis=1)
            QB[gi, rows, :] = (qf * lax.rsqrt(ssq * (1.0 / 64) + EPS) * qg).astype(BF16)
            kv = a[:, 1024:1152].astype(BF16).astype(F32)
            is_key = lax.broadcasted_iota(jnp.int32, (128, 128), 1) < 64
            ksq = jnp.sum(jnp.where(is_key, kv * kv, 0.0), axis=-1, keepdims=True)
            kn = kv * lax.rsqrt(ksq * (1.0 / 64) + EPS) * PRM[0, 12:13, :]
            KV[gi, slot, pl.ds(pl.multiple_of(128 + r * 128, 128), 128), :] = jnp.where(
                is_key, kn, kv
            ).astype(BF16)
            return carry

        lax.fori_loop(0, 4, body, 0)

    def holder(q, c_):
        inner = lax.rem(lax.div(q + 1, 2), 2)
        even = lax.div(q, 2) * 2 + par
        odd = inner * (2 - par) + (1 - inner) * 3 * par
        return (1 - c_) * even + c_ * odd

    quarters = (x, p)

    def halo_next(gi, i):
        q = quarters[i]
        qn = mod4(q + 1)
        spn = sp + lax.div(q + 1, 4)
        xn = holder(qn, lax.rem(spn, 2))
        slot = jnp.where(xn == qn, 0, 1)
        gn = jnp.where(xn == x, gi, 1 - gi)
        here = (spn == sp) & (xn == x)
        away = jnp.logical_not(here) & (spn < 32)
        spn_ok = jnp.where(spn < 32, spn, 0)
        copies = [
            pltpu.make_async_remote_copy(
                src_ref=src, dst_ref=dst, send_sem=hsend.at[gi, i, k], recv_sem=hrecv.at[gn, slot, k],
                device_id=(spn_ok, xn), device_id_type=MESH,
            )
            for k, (src, dst) in enumerate(
                (
                    (KV.at[gi, i, pl.ds(256, 128)], KV.at[gn, slot, pl.ds(0, 128)]),
                    (PB.at[gi, i, pl.ds(256, 16)], PB.at[gn, slot, pl.ds(0, 16)]),
                )
            )
        ]
        return here, away, copies

    def halo_send(gi):
        for i in range(2):
            here, away, copies = halo_next(gi, i)

            @pl.when(away)
            def _():
                for d in copies:
                    d.start()

            @pl.when(here)
            def _():
                KV[gi, 1 - i, pl.ds(0, 128), :] = KV[gi, i, pl.ds(256, 128), :]
                PB[gi, 1 - i, pl.ds(0, 16), :] = PB[gi, i, pl.ds(256, 16), :]

    def halo_sent(gi):
        for i in range(2):
            _, away, copies = halo_next(gi, i)

            @pl.when(away)
            def _():
                for d in copies:
                    d.wait_send()

    def halo_wait(gi):
        for i in range(2):
            q = quarters[i]
            first = (sp == 0) & (q == 0)
            qp = mod4(q + 3)
            back = jnp.where(q == 0, 1, 0)
            spp = sp - back
            xp = holder(qp, lax.rem(spp + 2, 2))
            here = (back == 0) & (xp == x)

            @pl.when(first)
            def _():
                KV[gi, i, pl.ds(0, 128), :] = jnp.zeros((128, 128), BF16)
                PB[gi, i, pl.ds(0, 16), :] = jnp.zeros((16, 512), BF16)

            @pl.when(jnp.logical_not(first) & jnp.logical_not(here))
            def _():
                for k, dst in enumerate((KV.at[gi, i, pl.ds(0, 128)], PB.at[gi, i, pl.ds(0, 16)])):
                    pltpu.make_async_copy(dst, dst, hrecv.at[gi, i, k]).wait()

    def pool(gi, g):
        span = lax.shift_left(jnp.int32(2), g)
        for i in range(2):
            pf = PB[gi, i].astype(F32)
            t2 = pf + pltpu.roll(pf, 1, 0)
            t4 = t2 + pltpu.roll(t2, 2, 0)
            t8 = t4 + pltpu.roll(t4, 4, 0)
            t16 = t8 + pltpu.roll(t8, 8, 0)
            run = jnp.where(g == 0, t2, jnp.where(g == 1, t4, jnp.where(g == 2, t8, t16)))[16:]
            pos = sp * 1024 + quarters[i] * 256 + lax.broadcasted_iota(jnp.int32, (256, 1), 0)
            count = jnp.minimum(pos + 1, span).astype(F32)
            diff = (run * (1.0 / count) - pf[16:]).astype(BF16)
            m = jnp.dot(diff, PM[gi], preferred_element_type=F32)
            m = m * jnp.concatenate([PRM[gi, j : j + 1, :] for j in range(4)], axis=1)
            m = m * lax.rsqrt(jnp.mean(m * m, axis=-1, keepdims=True) + EPS)
            MIX[gi, i * 256 : (i + 1) * 256, 0:512] = m.astype(BF16)

    def attend(gi):
        es = jnp.exp(PRM[gi, 4:8, :])
        es = jnp.concatenate(
            [jnp.broadcast_to(es[j : j + 1], (128, 128)) for j in range(4)], axis=0
        )

        def body(k, carry):
            slot, r = lax.div(k, 2), lax.rem(k, 2)
            rows = pl.ds(pl.multiple_of(k * 128, 128), 128)
            kv = KV[gi, slot, pl.ds(pl.multiple_of(r * 128, 128), 256), :].astype(F32)
            low = lax.broadcasted_iota(jnp.int32, (256, 128), 1) < 64
            ke = jnp.where(low, kv, 0.0)
            vo = jnp.where(low, 0.0, kv)
            ko = pltpu.roll(ke, 64, 1)
            ve = pltpu.roll(vo, 64, 1)
            q_here = (1 - slot) * x + slot * p
            missing = jnp.where((sp == 0) & (q_here == 0) & (r == 0), 128, 0)
            there = lax.broadcasted_iota(jnp.int32, (256, 128), 0) >= missing
            oe = jnp.where(low & there, 1.0, 0.0)
            oo = jnp.where(jnp.logical_not(low) & there, 1.0, 0.0)
            keys = jnp.concatenate([ke, ko], axis=0).astype(BF16)
            values = jnp.concatenate(
                [jnp.concatenate([ve, oe], axis=1), jnp.concatenate([vo, oo], axis=1)], axis=0
            ).astype(BF16)
            q = QB[gi, rows, :]
            q = jnp.concatenate([q[:, j * 128 : (j + 1) * 128] for j in range(4)], axis=0)
            sc = lax.dot_general(q, keys, (((1,), (1,)), ((), ())), preferred_element_type=F32)
            e = jnp.exp(sc + BIAS[gi]).astype(BF16)
            o = jnp.dot(e, values, preferred_element_type=F32)
            att = o[:, 0:128] / (o[:, 128:256] + es)
            parts = [att[j * 128 : (j + 1) * 128] for j in range(4)]
            sq = parts[0] * parts[0]
            for j in range(1, 4):
                sq += parts[j] * parts[j]
            r_ = lax.rsqrt(jnp.sum(sq, axis=-1, keepdims=True) * (1.0 / 512) + EPS)
            for j in range(4):
                MIX[gi, rows, 512 + j * 128 : 640 + j * 128] = (parts[j] * r_).astype(BF16)
            return carry

        lax.fori_loop(0, 4, body, 0)

    step_e1(0, d1, sib1)
    recv(*sib1)
    order = lambda t: jnp.where(t == 0, x, jnp.where(t == 1, p, jnp.where(t == 2, n, x2)))
    body0 = matmuls(0, order)
    lax.fori_loop(0, 3, body0, 0)
    recv(*tf)
    scale_slab(x2)
    lax.fori_loop(3, 4, body0, 0)
    post(0)
    halo_send(0)
    step_e1(1, d1o, sib1o)
    recv(*sib1o)
    body1 = matmuls(1, order)
    lax.fori_loop(0, 4, body1, 0)
    post(1)
    halo_send(1)

    recv(sib_pm)
    halo_wait(0)
    attend(0)
    pool(0, x)
    halo_wait(1)
    attend(1)
    pool(1, x2)

    def unit(u, cc, s_, k):
        rhs = []
        for g in range(2):
            rhs.append(
                jnp.concatenate([W2[cc, s_, 2 * k, g], W2[cc, s_, 2 * k + 1, g]], axis=1)
            )
        o = jnp.dot(MIX[0], rhs[0], preferred_element_type=F32)
        o += jnp.dot(MIX[1], rhs[1], preferred_element_type=F32)
        ob = o.astype(BF16)
        for e in range(2):
            idx = 2 * u + e
            f_ = 2 * k + e
            col = pl.ds(pl.multiple_of(sp_of(cc, f_, s_) * 128, 128), 128)
            OWNB[idx] = ob[0:256, e * 128 : (e + 1) * 128]
            SENDB[idx] = ob[256:512, e * 128 : (e + 1) * 128]
            out_copy(idx, col).start()
            pltpu.make_async_copy(OWNB.at[idx], own_out.at[:, col], oloc.at[idx]).start()

    def out_copy(idx, col):
        return pltpu.make_async_remote_copy(
            src_ref=SENDB.at[idx], dst_ref=recv_out.at[:, col], send_sem=osend.at[idx],
            recv_sem=orecv.at[idx], device_id=dev_p, device_id_type=MESH,
        )

    def pair(stage, mine, sA, kA, sB, kB):
        cc = c if mine else cs

        def body(t, carry):
            unit(stage * 4 + (0 if mine else 2) + t, cc, sA + t * (sB - sA), kA + t * (kB - kA))
            return carry

        lax.fori_loop(0, 2, body, 0)

    pair(0, True, s, 0, s, 1)
    recv(*sib2_own)
    pair(0, False, ss_, 0, ss_, 1)

    recv(*c2a)
    u0, d0 = half_plane(sd, 0), half_plane(su, 1)
    d2 = [send(u0, u0, dev_su), send(d0, d0, dev_sd)]
    sib2_a = [send(u0, u0, dev_sib), send(d0, d0, dev_sib)]
    pair(1, True, sd, 0, su, 1)
    recv(*sib2_a)
    pair(1, False, ssd, 0, ssu, 1)

    recv(*c2b)
    u1, d1_ = half_plane(sd, 1), half_plane(su, 0)
    sib2_b = [send(u1, u1, dev_sib), send(d1_, d1_, dev_sib)]
    pair(2, True, sd, 1, su, 0)
    recv(*sib2_b)
    pair(2, False, ssd, 1, ssu, 0)

    recv(*d2)
    u2, d2_ = half_plane(s2, 0), half_plane(s2, 1)
    sib2_c = [send(u2, u2, dev_sib), send(d2_, d2_, dev_sib)]
    pair(3, True, s2, 0, s2, 1)
    recv(*sib2_c)
    pair(3, False, ss2, 0, ss2, 1)

    tf_ids = {id(d) for d in tf}
    for d in pending:
        if id(d) not in tf_ids:
            d.wait_send()
    halo_sent(0)
    halo_sent(1)

    def drain(idx, carry):
        col = pl.ds(pl.multiple_of(idx * 128, 128), 128)
        d = out_copy(idx, col)
        d.wait_send()
        d.wait_recv()
        pltpu.make_async_copy(OWNB.at[idx], own_out.at[:, col], oloc.at[idx]).wait()
        return carry

    lax.fori_loop(0, 32, drain, 0)


def local_program(
    tokens, norm_gain, w_pool_in, w_query, w_key, w_value, pool_map, pool_scale,
    q_gain, k_gain, sinks, w_out,
):
    wkv = jnp.concatenate([w_key, w_value], axis=1)
    prm = jnp.concatenate(
        [
            pool_scale,
            jnp.repeat(sinks, 64),
            jnp.tile(q_gain * 0.125, 8),
            k_gain,
            jnp.ones((64,), F32),
            jnp.zeros((3 * 128,), F32),
        ]
    ).reshape(16, 128)
    any_ = pl.BlockSpec(memory_space=pl.ANY)
    vmem = pl.BlockSpec(memory_space=pltpu.VMEM)
    dma = pltpu.SemaphoreType.DMA
    own, got = pl.pallas_call(
        kernel,
        out_shape=[jax.ShapeDtypeStruct((256, 4096), BF16)] * 2,
        in_specs=[any_] * 7 + [vmem],
        out_specs=[any_, any_],
        scratch_shapes=[
            pltpu.VMEM((2, 2, 4, 4, 128, 1152), BF16),
            pltpu.VMEM((2, 4, 4, 2, 1024, 128), BF16),
            pltpu.VMEM((2, 4, 256, 1024), BF16),
            pltpu.VMEM((128, 1152), BF16),
            pltpu.VMEM((1024, 128), BF16),
            pltpu.VMEM((256, 512), BF16),
            pltpu.VMEM((2, 512, 512), BF16),
            pltpu.VMEM((2, 16, 128), F32),
            pltpu.VMEM((2, 2, 384, 128), BF16),
            pltpu.VMEM((2, 2, 272, 512), BF16),
            pltpu.VMEM((2, 512, 512), BF16),
            pltpu.VMEM((512, 1152), F32),
            pltpu.VMEM((2, 256, 128), F32),
            pltpu.VMEM((2, 512, 1024), BF16),
            pltpu.VMEM((2, 512, 512), F32),
            pltpu.VMEM((512, 512), BF16),
            pltpu.VMEM((32, 256, 128), BF16),
            pltpu.VMEM((32, 256, 128), BF16),
            dma((8,)),
            dma((N_COPIES,)),
            dma((N_COPIES,)),
            dma((32,)),
            dma((32,)),
            dma((32,)),
            dma((2, 2, 2)),
            dma((2, 2, 2)),
        ],
        compiler_params=pltpu.CompilerParams(
            has_side_effects=True, vmem_limit_bytes=66_000_000
        ),
        name="mixer",
    )(tokens, w_pool_in, w_query, wkv, w_out, pool_map.reshape(512, 512), prm, norm_gain.reshape(1, 4096))
    return (own.astype(F32) + got.astype(F32)).astype(BF16)


def solution(mesh):
    in_specs = (
        P("sp", "tp"), P(), P("sp", "tp"), P("sp", "tp"), P("sp", "tp"), P("sp", "tp"),
        P("tp", None, None), P("tp"), P(), P(), P("tp"), P("tp", "sp"),
    )
    out_specs = P(("sp", "tp"), None)
    return jax.shard_map(local_program, mesh=mesh, in_specs=in_specs, out_specs=out_specs, check_vma=False)
```

time: 285 us -> 172 us (0.60)
  waiting for transfers between devices: 172 us -> 0 us
  Pallas kernels: 0 us -> 162 us
  matrix products: 39.4 us -> 0 us
  local copies, waits for them, and re-layouts: 22.2 us -> 3.89 us
  other arithmetic: 23 us -> 5.7 us
  between operations: 13.6 us -> 0.02 us
  starting transfers between devices: 13.3 us -> 0 us
    pallas_call x0 -> x1, Pallas kernels: none -> 162 us  [local_program(): pl.pallas_call(kernel, out_shape=[jax.ShapeDtypeStruct((256, 4096), BF16)...]
    all_to_all x1 -> x0, waiting for transfers between devices: 91.2 us -> none  [copy_for_each(): return lax.all_to_all(copies, axis, split_axis=0, concat_axis=0, tiled=True)]
    reduce_scatter x1 -> x0, waiting for transfers between devices: 80.5 us -> none  [local(): lax.psum_scatter(jnp.dot(mixed_rows, out_columns, preferred_element_type=...]
    dot_general x8 -> x0, matrix products: 39.4 us -> none  [the longest x4 18.3 us: local(): jnp.dot(normed, weight_piece, preferred_element_type=jnp.float32)]
    ppermute x2 -> x0, starting transfers between devices: 7.42 us -> none  [passed_along(): lax.ppermute(value, axis, [(source, source + steps) for source in range(f...]
    reduce_sum x3 -> x0, other arithmetic: 7.22 us -> none  [rms_scale(): jnp.mean(values * values, axis=-1, keepdims=True) + epsilon]
    all_to_all x1 -> x0, starting transfers between devices: 5.75 us -> none  [copy_for_each(): return lax.all_to_all(copies, axis, split_axis=0, concat_axis=0, tiled=True)]
    unnamed x32 -> x2, local copies, waits for them, and re-layouts: 7.27 us -> 1.66 us
  transfers between devices with their start and end apart: 6 -> 0, of which waited for: 2 -> 0; matrix products, arithmetic and copies ran while one was open for 23% -> 0% of each run, Pallas kernels for 0% -> 0%
where the time goes in v1:
time: 172 us; the launch traced here: 171 us
  Pallas kernels  162 us (94%)
  other arithmetic  5.7 us (3%)
  local copies, waits for them, and re-layouts  3.89 us (2%)
    pallas_call x1, Pallas kernels, local_program(): pl.pallas_call(kernel, out_shape=[jax.ShapeDtypeStruct((256, 4096), BF16)...  162 us
    convert_element_type x1, other arithmetic, local_program(): return (own.astype(F32) + got.astype(F32)).astype(BF16)  4.33 us

profile of v1, /device:TPU:1, one launch (start us, length us, event | category | flops | bytes accessed | tf_op | source)
XLA Modules:
  0.0 171.3 jit_solution(12271188419685570402)
XLA Ops:
  0.0 0.7 broadcast_multiply_fusion
  0.7 0.1 tile.10
  0.7 0.7 broadcast_in_dim.9
  1.5 0.1 reshape.14
  1.5 1.3 concatenate.7
  2.9 0.8 copy.13
  3.7 0.8 copy.14
  4.6 0.7 pad_maximum_fusion.wkv
  5.3 161.7 %mixer.1 = (bf16[256,4096]{1,0:T(8,128)(2,1)}, bf16[256,4096]{1,0:T(8,128)(2,1)}) custom-call(bf16[1024,1024]{1,0:T(8,128)(2,1)} %tokens.1, bf16[128,512]{1,0:T(8,128)(2,1)} %wp.1, bf16[128,512]{1,0:T(8,128)(2,1)} %wq.1, bf16[128,128]{1,0:T(8,128)(2,1)} %pad_maximum_fusion.wkv, bf16[1024,128]{1,0:T(8,128)(2,1)} %wo.1, bf16[512,512]{1,0:T(8,128)(2,1)} %bitcast.3, ...), custom_call_target="tpu_custom_call" | custom-call | tf_op jit(solution)/shard_map/mixer/pallas_call | solution.py:523
  167.0 4.3 %add_convert_fusion = bf16[256,4096]{1,0:T(8,128)(2,1)} fusion(bf16[256,4096]{1,0:T(8,128)(2,1)} %get-tuple-element.8, bf16[256,4096]{1,0:T(8,128)(2,1)} %get-tuple-element.7), kind=kLoop, calls=%fused_computation | loop fusion | flops 4194304 | bytes 6291456 | tf_op jit(solution)/shard_map/convert_element_type | solution.py:561
  (3 shorter events, 0.0 us)

commit v2 on v1

v2 whole, which is shorter than its diff:
```python
import jax
import jax.numpy as jnp
from jax import lax
from jax.experimental import pallas as pl
from jax.experimental.pallas import tpu as pltpu
from jax.sharding import PartitionSpec as P

MESH = pl.DeviceIdType.MESH
F32 = jnp.float32
BF16 = jnp.bfloat16
EPS = 1e-6
N_COPIES = 128


def mod4(v):
    return lax.rem(v, 4)


def kernel(
    tokens, wp, wq, wk_t, wv_t, wo, pmap, scale_in, sinks_in, q_gain, k_gain, gain,
    out,
    W1, W2, TOK, ST1, ST2, ST3, PM, SCALE, SINK, KVT, KV, PB, QB, ACC, SS, MIX, BIAS, BLK, SENDB, OWNB, RECVB, RLK, RLP,
    lsem, ssem, rsem, osend, orecv, oloc, hsend, hrecv, rlsend, rlrecv,
):
    sp = lax.axis_index("sp")
    x = lax.axis_index("tp")
    c = lax.rem(sp, 2)
    y = mod4(lax.div(sp, 2))
    z = lax.div(sp, 8)
    f = y + c * (z - y)
    s = z + c * (y - z)
    par = lax.rem(x, 2)
    flip1 = x + 1 - 2 * par
    flip3 = 3 - x
    p = (1 - c) * flip1 + c * flip3
    n = (1 - c) * flip3 + c * flip1
    x2 = mod4(x + 2)
    dx = mod4(x + 1 + 2 * c)

    def sp_of(c_, f_, s_):
        y_ = (1 - c_) * f_ + c_ * s_
        z_ = (1 - c_) * s_ + c_ * f_
        return (z_ * 4 + y_) * 2 + c_

    fu, fd = mod4(f + 1), mod4(f + 3)
    su, sd, s2 = mod4(s + 1), mod4(s + 3), mod4(s + 2)
    dev_fu, dev_fd = (sp_of(c, fu, s), x), (sp_of(c, fd, s), x)
    dev_su, dev_sd = (sp_of(c, f, su), x), (sp_of(c, f, sd), x)
    dev_sib = (sp + 1 - 2 * c, x)
    dev_dx, dev_p, dev_n, dev_x2 = (sp, dx), (sp, p), (sp, n), (sp, x2)
    cs, ss_, sf_ = 1 - c, f, s
    ssu, ssd, ss2 = mod4(ss_ + 1), mod4(ss_ + 3), mod4(ss_ + 2)

    pending = []

    def send(src, dst, dev):
        k = len(pending)
        d = pltpu.make_async_remote_copy(
            src_ref=src, dst_ref=dst, send_sem=ssem.at[k], recv_sem=rsem.at[k],
            device_id=dev, device_id_type=MESH,
        )
        d.start()
        pending.append(d)
        return d

    def recv(*ds):
        for d in ds:
            d.wait_recv()

    loc = []

    def local(src, dst):
        d = pltpu.make_async_copy(src, dst, lsem.at[len(loc)])
        d.start()
        loc.append(d)
        return d

    own1 = W1.at[0, c, s, f]
    l0 = local(wp, own1.at[:, pl.ds(0, 512)])
    l1 = local(wq, own1.at[:, pl.ds(512, 512)])
    l2 = local(wk_t, KVT.at[pl.ds(0, 64)])
    l7 = local(wv_t, KVT.at[pl.ds(64, 64)])
    l3 = local(wo, W2.at[c, s, f, 0])
    l4 = local(tokens.at[pl.ds(x * 256, 256)], TOK.at[0, x])
    l5 = local(tokens.at[pl.ds(p * 256, 256)], TOK.at[1, x])
    l6 = local(pmap, PM.at[0])

    def holder(q, c_):
        inner = lax.rem(lax.div(q + 1, 2), 2)
        even = lax.div(q, 2) * 2 + par
        odd = inner * (2 - par) + (1 - inner) * 3 * par
        return (1 - c_) * even + c_ * odd

    quarters = (x, p)

    def halo_to(i):
        q = quarters[i]
        qn = mod4(q + 1)
        spn = sp + lax.div(q + 1, 4)
        xn = holder(qn, lax.rem(spn, 2))
        here = (spn == sp) & (xn == x)
        away = jnp.logical_not(here) & (spn < 32)
        passed = away & (c == 1) & (q == 3)
        return qn, jnp.where(spn < 32, spn, 0), xn, here, away & jnp.logical_not(passed), passed

    def halo_from(i):
        q = quarters[i]
        first = (sp == 0) & (q == 0)
        back = jnp.where(q == 0, 1, 0)
        relayed = (back == 1) & (c == 0)
        spp = jnp.where(first, sp, sp - back - jnp.where(relayed, 1, 0))
        xp = holder(mod4(q + 3), lax.rem(sp - back + 2, 2))
        here = (back == 0) & (xp == x)
        return first, jnp.logical_not(first) & jnp.logical_not(here), spp, xp

    relay = (c == 0) & ((x == 0) | (x == 3)) & (sp < 30)
    relay_dev = (jnp.where(relay, sp + 2, 0), par)
    relay_slot = jnp.where(par == 0, 0, 1)

    barrier = pltpu.get_barrier_semaphore()

    def greet(dev):
        pl.semaphore_signal(barrier, inc=1, device_id=dev, device_id_type=MESH)

    for dev in (dev_fu, dev_fd, dev_su, dev_sd, dev_sib, dev_p, dev_n, dev_x2):
        greet(dev)
    @pl.when(relay)
    def _():
        greet(relay_dev)

    for i in range(2):
        _, spn, xn, _, away, _ = halo_to(i)

        @pl.when(away)
        def _():
            greet((spn, xn))

        _, apart, spp, xp = halo_from(i)

        @pl.when(apart)
        def _():
            greet((spp, xp))

    lane_i = lax.broadcasted_iota(jnp.int32, (512, 512), 1)
    row_i = lax.broadcasted_iota(jnp.int32, (512, 512), 0)
    l2.wait()
    l7.wait()
    W1[0, c, s, f, :, pl.ds(1024, 128)] = KVT[...].astype(F32).T.astype(BF16)
    BLK[...] = jnp.where(
        lax.shift_right_logical(lane_i, 6) == lax.shift_right_logical(row_i, 6), 1.0, 0.0
    ).astype(BF16)
    SS[...] = jnp.zeros_like(SS)
    key_i = jnp.bitwise_and(lane_i, 255)
    dist = 128 + jnp.bitwise_and(row_i, 127) - key_i
    band = (dist >= 0) & (dist < 128)
    head_in = 2 * lax.shift_right_logical(row_i, 7) + lax.shift_right_logical(lane_i, 8) + 1
    for gi, g in ((0, x), (1, x2)):
        slope = jnp.exp2(-0.25 * (g * 8 + head_in).astype(F32))
        BIAS[gi] = jnp.where(band, -slope * dist.astype(F32), -1e30)

    peers = 8 + jnp.where(relay, 1, 0)
    for i in range(2):
        peers += jnp.where(halo_to(i)[4], 1, 0) + jnp.where(halo_from(i)[1], 1, 0)
    pl.semaphore_wait(barrier, peers)

    l0.wait()
    l1.wait()
    l3.wait()
    def halves(src, dst, dev, first):
        return [
            send(src.at[pl.ds(r, 64)], dst.at[pl.ds(r, 64)], dev) for r in (first, 64 - first)
        ]

    def step_a1(g):
        piece = W1.at[g, c, s, f]
        up, down = halves(piece, piece, dev_fu, 0), halves(piece, piece, dev_fd, 64)
        return [up[0], down[0]], [up[1], down[1]]

    def step_b1(g, a):
        recv(*a[0])
        lo, hi = W1.at[g, c, s, fd, pl.ds(0, 64)], W1.at[g, c, s, fu, pl.ds(64, 64)]
        return [send(lo, lo, dev_fu), send(hi, hi, dev_fd)]

    def step_c1(g, a, b):
        recv(*a[1], *b)
        plane = W1.at[g, c, s]
        lo, hi = plane.at[pl.ds(0, 2)], plane.at[pl.ds(2, 2)]
        first = [send(lo, lo, dev_su), send(hi, hi, dev_sd)]
        second = [send(hi, hi, dev_su), send(lo, lo, dev_sd)]
        return first, second, [send(plane, plane, dev_sib)]

    def step_d1(g, cc):
        recv(*cc[0])
        lo, hi = W1.at[g, c, sd, pl.ds(0, 2)], W1.at[g, c, su, pl.ds(2, 2)]
        return [send(lo, lo, dev_su), send(hi, hi, dev_sd)]

    def share1(g, s_):
        piece = W1.at[g, c, s_]
        return send(piece, piece, dev_sib)

    def step_a2(g):
        piece = W2.at[c, s, f, g]
        return [send(piece, piece, dev_fu), send(piece, piece, dev_fd)]

    def step_b2(g, a):
        recv(*a)
        lo, hi = W2.at[c, s, fd, g, pl.ds(0, 512)], W2.at[c, s, fu, g, pl.ds(512, 512)]
        return [send(lo, lo, dev_fu), send(hi, hi, dev_fd)]

    x_w1 = halves(own1, ST1, dev_dx, 0)
    a1 = step_a1(0)
    a2 = step_a2(0)
    x_w2 = send(W2.at[c, s, f, 0], ST2, dev_dx)

    f_w1 = []
    b1 = None
    for k in range(2):
        recv(x_w1[k])
        part = pl.ds(64 * k, 64)
        f_w1.append(send(ST1.at[part], W1.at[1, c, s, f, part], dev_dx))
        if k == 0:
            b1 = step_b1(0, a1)
    c1a, c1b, sib1 = step_c1(0, a1, b1)
    recv(x_w2)
    f_w2 = send(ST2, W2.at[c, s, f, 1], dev_dx)
    tn = [
        send(tokens.at[pl.ds(n * 256, 256)], TOK.at[0, x], dev_n),
        send(tokens.at[pl.ds(x2 * 256, 256)], TOK.at[1, x], dev_n),
    ]
    sc_c = [send(scale_in, SCALE, dev_x2), send(sinks_in, SINK, dev_x2)]

    recv(*f_w1)
    a1o = step_a1(1)

    def scale_slab(j):
        g = gain[:, pl.ds(pl.multiple_of(j * 1024, 1024), 1024)]

        def body(k, carry):
            slot, r = lax.div(k, 4), pl.ds(lax.rem(k, 4) * 64, 64)
            t = TOK[slot, j, r, :].astype(F32)
            sq = t * t
            tot = sq[:, 0:128]
            for m in range(1, 8):
                tot += sq[:, m * 128 : (m + 1) * 128]
            SS[slot, r, :] += tot
            TOK[slot, j, r, :] = (t * g).astype(BF16)
            return carry

        lax.fori_loop(0, 8, body, 0)

    l4.wait()
    l5.wait()
    scale_slab(x)
    b1o = step_b1(1, a1o)
    recv(f_w2)
    a2o = step_a2(1)
    b2 = step_b2(0, a2)
    d1 = step_d1(0, (c1a, c1b))
    c1oa, c1ob, sib1o = step_c1(1, a1o, b1o)
    tp_ = [
        send(tokens.at[pl.ds(p * 256, 256)], TOK.at[0, x], dev_p),
        send(tokens.at[pl.ds(x * 256, 256)], TOK.at[1, x], dev_p),
    ]
    recv(*c1b)
    sib1 += [share1(0, sd), share1(0, su)]
    recv(*tn)
    tf = [
        send(TOK.at[0, n], TOK.at[1, n], dev_p),
        send(TOK.at[1, n], TOK.at[0, n], dev_p),
    ]
    l6.wait()
    half = pl.ds(c * 256, 256)
    x_pm = send(PM.at[0, half], ST3, dev_dx)
    b2o = step_b2(1, a2o)

    def half_plane(s_, k):
        return W2.at[c, s_, pl.ds(2 * k, 2)]

    def c2_send(k_up, k_dn):
        u, d = half_plane(s, k_up), half_plane(s, k_dn)
        return [send(u, u, dev_su), send(d, d, dev_sd)]

    def matmul(gi, jz):
        parts = []
        for yy in range(4):
            parts.append(W1[gi, 0, jz, yy])
            parts.append(W1[gi, 1, yy, jz])
        rhs = jnp.concatenate(parts, axis=0)
        lhs = TOK[:, jz].reshape(512, 1024)
        ACC[...] += jnp.dot(lhs, rhs, preferred_element_type=F32)

    def matmul_slab(gi, jz):
        lax.fori_loop(0, 1, lambda t, carry: (matmul(gi, jz), carry)[1], 0)

    def matmul_planes(gi, cc, sA, sB, count):
        def body(t, carry):
            s_ = sA + t * (sB - sA)
            rhs = jnp.concatenate([W1[gi, cc, s_, k] for k in range(4)], axis=0)
            lhs = []
            for k in range(4):
                off = ((1 - cc) * k + cc * s_) * 256 + cc * 128
                col = pl.ds(pl.multiple_of(off, 128), 128)
                lhs.append(TOK[:, (1 - cc) * s_ + cc * k, :, col].reshape(512, 128))
            lhs = jnp.concatenate(lhs, axis=1)
            ACC[...] += jnp.dot(lhs, rhs, preferred_element_type=F32)
            return carry

        lax.fori_loop(0, count, body, 0)

    def post(gi):
        def body(k, carry):
            slot, r = lax.div(k, 2), lax.rem(k, 2)
            rows = pl.ds(pl.multiple_of(k * 128, 128), 128)
            tot = jnp.sum(SS[slot, pl.ds(r * 128, 128), :], axis=-1, keepdims=True)
            a = ACC[rows, :] * lax.rsqrt(tot * (1.0 / 4096) + EPS)
            PB[gi, slot, pl.ds(pl.multiple_of(16 + r * 128, 16), 128), :] = a[:, 0:512].astype(BF16)
            qf = a[:, 512:1024].astype(BF16).astype(F32)
            sq = qf * qf
            hi = sq.astype(BF16)
            lo = (sq - hi.astype(F32)).astype(BF16)
            ssq = jnp.dot(hi, BLK[...], preferred_element_type=F32) + jnp.dot(
                lo, BLK[...], preferred_element_type=F32
            )
            qg = jnp.concatenate([q_gain[...]] * 8, axis=1) * 0.125
            QB[gi, rows, :] = (qf * lax.rsqrt(ssq * (1.0 / 64) + EPS) * qg).astype(BF16)
            kv = a[:, 1024:1152].astype(BF16).astype(F32)
            is_key = lax.broadcasted_iota(jnp.int32, (128, 128), 1) < 64
            ksq = jnp.sum(jnp.where(is_key, kv * kv, 0.0), axis=-1, keepdims=True)
            kn = kv * lax.rsqrt(ksq * (1.0 / 64) + EPS) * jnp.concatenate([k_gain[...]] * 2, axis=1)
            KV[gi, slot, pl.ds(pl.multiple_of(128 + r * 128, 128), 128), :] = jnp.where(
                is_key, kn, kv
            ).astype(BF16)
            return carry

        lax.fori_loop(0, 4, body, 0)

    def halo_next(gi, i):
        qn, spn, xn, here, away, passed = halo_to(i)
        slot = jnp.where(xn == qn, 0, 1)
        gn = jnp.where(xn == x, gi, 1 - gi)
        tails = (KV.at[gi, i, pl.ds(256, 128)], PB.at[gi, i, pl.ds(256, 16)])
        copies = [
            pltpu.make_async_remote_copy(
                src_ref=src, dst_ref=dst, send_sem=hsend.at[gi, i, k], recv_sem=hrecv.at[gn, slot, k],
                device_id=(spn, xn), device_id_type=MESH,
            )
            for k, (src, dst) in enumerate(
                zip(tails, (KV.at[gn, slot, pl.ds(0, 128)], PB.at[gn, slot, pl.ds(0, 16)]))
            )
        ]
        passes = [
            pltpu.make_async_remote_copy(
                src_ref=src, dst_ref=dst, send_sem=hsend.at[gi, i, k], recv_sem=rlrecv.at[gi, k],
                device_id=dev_sib, device_id_type=MESH,
            )
            for k, (src, dst) in enumerate(zip(tails, (RLK.at[gi], RLP.at[gi])))
        ]
        return here, away, copies, passed, passes

    def halo_send(gi):
        for i in range(2):
            here, away, copies, passed, passes = halo_next(gi, i)

            @pl.when(passed)
            def _():
                for d in passes:
                    d.start()

            @pl.when(away)
            def _():
                for d in copies:
                    d.start()

            @pl.when(here)
            def _():
                KV[gi, 1 - i, pl.ds(0, 128), :] = KV[gi, i, pl.ds(256, 128), :]
                PB[gi, 1 - i, pl.ds(0, 16), :] = PB[gi, i, pl.ds(256, 16), :]

    def halo_sent(gi):
        for i in range(2):
            _, away, copies, passed, passes = halo_next(gi, i)

            @pl.when(passed)
            def _():
                for d in passes:
                    d.wait_send()

            @pl.when(away)
            def _():
                for d in copies:
                    d.wait_send()

    def relay_copies(gi):
        gn = jnp.where(par == x, gi, 1 - gi)
        return [
            pltpu.make_async_remote_copy(
                src_ref=src, dst_ref=dst, send_sem=rlsend.at[gi, k],
                recv_sem=hrecv.at[gn, relay_slot, k], device_id=relay_dev, device_id_type=MESH,
            )
            for k, (src, dst) in enumerate(
                (
                    (RLK.at[gi], KV.at[gn, relay_slot, pl.ds(0, 128)]),
                    (RLP.at[gi], PB.at[gn, relay_slot, pl.ds(0, 16)]),
                )
            )
        ]

    def halo_relay(gi):
        @pl.when(relay)
        def _():
            for k, dst in enumerate((RLK.at[gi], RLP.at[gi])):
                pltpu.make_async_copy(dst, dst, rlrecv.at[gi, k]).wait()
            for d in relay_copies(gi):
                d.start()

    def relay_sent(gi):
        @pl.when(relay)
        def _():
            for d in relay_copies(gi):
                d.wait_send()

    def halo_wait(gi):
        for i in range(2):
            first, apart, _, _ = halo_from(i)

            @pl.when(first)
            def _():
                KV[gi, i, pl.ds(0, 128), :] = jnp.zeros((128, 128), BF16)
                PB[gi, i, pl.ds(0, 16), :] = jnp.zeros((16, 512), BF16)

            @pl.when(apart)
            def _():
                for k, dst in enumerate((KV.at[gi, i, pl.ds(0, 128)], PB.at[gi, i, pl.ds(0, 16)])):
                    pltpu.make_async_copy(dst, dst, hrecv.at[gi, i, k]).wait()

    def pool(gi, g):
        span = lax.shift_left(jnp.int32(2), g)
        for i in range(2):
            pf = PB[gi, i].astype(F32)
            t2 = pf + pltpu.roll(pf, 1, 0)
            t4 = t2 + pltpu.roll(t2, 2, 0)
            t8 = t4 + pltpu.roll(t4, 4, 0)
            t16 = t8 + pltpu.roll(t8, 8, 0)
            run = jnp.where(g == 0, t2, jnp.where(g == 1, t4, jnp.where(g == 2, t8, t16)))[16:]
            pos = sp * 1024 + quarters[i] * 256 + lax.broadcasted_iota(jnp.int32, (256, 1), 0)
            count = jnp.minimum(pos + 1, span).astype(F32)
            diff = (run * (1.0 / count) - pf[16:]).astype(BF16)
            m = jnp.dot(diff, PM[gi], preferred_element_type=F32)
            m = m * (scale_in if gi == 0 else SCALE)[...]
            m = m * lax.rsqrt(jnp.mean(m * m, axis=-1, keepdims=True) + EPS)
            MIX[gi, i * 256 : (i + 1) * 256, 0:512] = m.astype(BF16)

    def attend(gi, r):
        sink = jnp.exp((sinks_in if gi == 0 else SINK)[...])
        left = lax.broadcasted_iota(jnp.int32, (1, 128), 1) < 64
        es = jnp.concatenate(
            [
                jnp.broadcast_to(
                    jnp.where(left, sink[:, 2 * j : 2 * j + 1], sink[:, 2 * j + 1 : 2 * j + 2]),
                    (128, 128),
                )
                for j in range(4)
            ],
            axis=0,
        )

        def body(k, carry):
            slot = k
            rows = pl.ds(pl.multiple_of(k * 256 + r * 128, 128), 128)
            kv = KV[gi, slot, pl.ds(r * 128, 256), :].astype(F32)
            low = lax.broadcasted_iota(jnp.int32, (256, 128), 1) < 64
            ke = jnp.where(low, kv, 0.0)
            vo = jnp.where(low, 0.0, kv)
            ko = pltpu.roll(ke, 64, 1)
            ve = pltpu.roll(vo, 64, 1)
            q_here = (1 - slot) * x + slot * p
            missing = jnp.where((sp == 0) & (q_here == 0), 128, 0) if r == 0 else 0
            there = lax.broadcasted_iota(jnp.int32, (256, 128), 0) >= missing
            oe = jnp.where(low & there, 1.0, 0.0)
            oo = jnp.where(jnp.logical_not(low) & there, 1.0, 0.0)
            keys = jnp.concatenate([ke, ko], axis=0).astype(BF16)
            values = jnp.concatenate(
                [jnp.concatenate([ve, oe], axis=1), jnp.concatenate([vo, oo], axis=1)], axis=0
            ).astype(BF16)
            q = QB[gi, rows, :]
            q = jnp.concatenate([q[:, j * 128 : (j + 1) * 128] for j in range(4)], axis=0)
            sc = lax.dot_general(q, keys, (((1,), (1,)), ((), ())), preferred_element_type=F32)
            e = jnp.exp(sc + BIAS[gi]).astype(BF16)
            o = jnp.dot(e, values, preferred_element_type=F32)
            att = o[:, 0:128] / (o[:, 128:256] + es)
            parts = [att[j * 128 : (j + 1) * 128] for j in range(4)]
            sq = parts[0] * parts[0]
            for j in range(1, 4):
                sq += parts[j] * parts[j]
            r_ = lax.rsqrt(jnp.sum(sq, axis=-1, keepdims=True) * (1.0 / 512) + EPS)
            for j in range(4):
                MIX[gi, rows, 512 + j * 128 : 640 + j * 128] = (parts[j] * r_).astype(BF16)
            return carry

        lax.fori_loop(0, 2, body, 0)

    recv(*d1)
    sib1.append(share1(0, s2))
    ACC[...] = jnp.zeros_like(ACC)
    recv(*sib1)
    matmul_slab(0, x)
    recv(*tp_)
    scale_slab(p)
    matmul_slab(0, p)
    d1o = step_d1(1, (c1oa, c1ob))
    recv(*b2, *b2o)
    c2a = c2_send(0, 1)
    c2b = c2_send(1, 0)
    plane2 = W2.at[c, s]
    sib2_own = [send(plane2, plane2, dev_sib)]
    for d in tf:
        d.wait_send()
    scale_slab(n)
    matmul_slab(0, n)
    recv(*tf)
    scale_slab(x2)
    matmul_slab(0, x2)
    post(0)
    halo_send(0)
    recv(*c1ob)
    sib1o += [share1(1, sd), share1(1, su)]
    recv(x_pm)
    f_pm = send(ST3, PM.at[1, half], dev_dx)
    ACC[...] = jnp.zeros_like(ACC)
    matmul_planes(1, c, s, s, 1)
    matmul_planes(1, c, sd, su, 2)
    recv(*sib1o)
    matmul_planes(1, cs, ss_, ss_, 1)
    matmul_planes(1, cs, ssd, ssu, 2)
    halo_relay(0)
    attend(0, 1)
    recv(*d1o)
    sib1o_far = share1(1, s2)
    matmul_planes(1, c, s2, s2, 1)
    recv(sib1o_far)
    matmul_planes(1, cs, ss2, ss2, 1)
    post(1)
    halo_send(1)

    recv(*sc_c)
    attend(1, 1)
    halo_relay(1)
    recv(f_pm)
    sib_pm = send(PM.at[1, half], PM.at[1, half], dev_sib)
    halo_wait(0)
    attend(0, 0)
    pool(0, x)
    halo_wait(1)
    attend(1, 0)
    recv(sib_pm)
    pool(1, x2)
    recv(*c2a)
    u0, d0 = half_plane(sd, 0), half_plane(su, 1)
    d2 = [[send(u0.at[k], u0.at[k], dev_su), send(d0.at[k], d0.at[k], dev_sd)] for k in range(2)]
    sib2_a = [send(u0, u0, dev_sib), send(d0, d0, dev_sib)]

    def unit(u, cc, s_, fs):
        rhs = []
        for g in range(2):
            rhs.append(jnp.concatenate([W2[cc, s_, fs[0], g], W2[cc, s_, fs[1], g]], axis=1))
        o = jnp.dot(MIX[0], rhs[0], preferred_element_type=F32)
        o += jnp.dot(MIX[1], rhs[1], preferred_element_type=F32)
        ob = o.astype(BF16)
        for e in range(2):
            idx = 2 * u + e
            OWNB[idx] = ob[0:256, e * 128 : (e + 1) * 128]
            SENDB[idx] = ob[256:512, e * 128 : (e + 1) * 128]
            out_copy(idx).start()

    def out_copy(idx):
        return pltpu.make_async_remote_copy(
            src_ref=SENDB.at[idx], dst_ref=RECVB.at[idx], send_sem=osend.at[idx],
            recv_sem=orecv.at[idx], device_id=dev_p, device_id_type=MESH,
        )

    def total(u, cc, s_, fs):
        for e in range(2):
            idx = 2 * u + e
            col = pl.ds(pl.multiple_of(sp_of(cc, fs[e], s_) * 128, 128), 128)
            out_copy(idx).wait_recv()
            OWNB[idx] = (OWNB[idx].astype(F32) + RECVB[idx].astype(F32)).astype(BF16)
            pltpu.make_async_copy(OWNB.at[idx], out.at[:, col], oloc.at[idx]).start()

    def pair(stage, mine, sA, kA, sB, kB, act=unit):
        cc = c if mine else cs

        def body(t, carry):
            k = kA + t * (kB - kA)
            act(stage * 4 + (0 if mine else 2) + t, cc, sA + t * (sB - sA), (2 * k, 2 * k + 1))
            return carry

        lax.fori_loop(0, 2, body, 0)

    pair(0, True, s, 0, s, 1)
    recv(*sib2_own)
    pair(0, False, ss_, 0, ss_, 1)

    pair(1, True, sd, 0, su, 1)
    recv(*sib2_a)
    pair(1, False, ssd, 0, ssu, 1)
    recv(*c2b)
    u1, d1_ = half_plane(sd, 1), half_plane(su, 0)
    sib2_b = [send(u1, u1, dev_sib), send(d1_, d1_, dev_sib)]
    pair(2, True, sd, 1, su, 0)
    recv(*sib2_b)
    pair(2, False, ssd, 1, ssu, 0)

    pair(0, True, s, 0, s, 1, total)
    pair(0, False, ss_, 0, ss_, 1, total)
    for k in range(2):
        recv(*d2[k])
        far = [W2.at[c, s2, k], W2.at[c, s2, 2 + k]]
        sib2_c = [send(r, r, dev_sib) for r in far]
        unit(12 + 2 * k, c, s2, (k, 2 + k))
        recv(*sib2_c)
        unit(13 + 2 * k, cs, ss2, (k, 2 + k))
        if k == 0:
            pair(1, True, sd, 0, su, 1, total)
            pair(1, False, ssd, 0, ssu, 1, total)

    pair(2, True, sd, 1, su, 0, total)
    pair(2, False, ssd, 1, ssu, 0, total)
    for k in range(2):
        total(12 + 2 * k, c, s2, (k, 2 + k))
        total(13 + 2 * k, cs, ss2, (k, 2 + k))

    tf_ids = {id(d) for d in tf}
    for d in pending:
        if id(d) not in tf_ids:
            d.wait_send()
    for gi in range(2):
        halo_sent(gi)
        relay_sent(gi)

    def drain(idx, carry):
        out_copy(idx).wait_send()
        col = pl.ds(pl.multiple_of(idx * 128, 128), 128)
        pltpu.make_async_copy(OWNB.at[idx], out.at[:, col], oloc.at[idx]).wait()
        return carry

    lax.fori_loop(0, 32, drain, 0)


def local_program(
    tokens, norm_gain, w_pool_in, w_query, w_key, w_value, pool_map, pool_scale,
    q_gain, k_gain, sinks, w_out,
):
    any_ = pl.BlockSpec(memory_space=pl.ANY)
    vmem = pl.BlockSpec(memory_space=pltpu.VMEM)
    dma = pltpu.SemaphoreType.DMA
    return pl.pallas_call(
        kernel,
        out_shape=jax.ShapeDtypeStruct((256, 4096), BF16),
        in_specs=[any_] * 7 + [vmem] * 5,
        out_specs=any_,
        scratch_shapes=[
            pltpu.VMEM((2, 2, 4, 4, 128, 1152), BF16),
            pltpu.VMEM((2, 4, 4, 2, 1024, 128), BF16),
            pltpu.VMEM((2, 4, 256, 1024), BF16),
            pltpu.VMEM((128, 1152), BF16),
            pltpu.VMEM((1024, 128), BF16),
            pltpu.VMEM((256, 512), BF16),
            pltpu.VMEM((2, 512, 512), BF16),
            pltpu.VMEM((1, 512), F32),
            pltpu.VMEM((1, 8), F32),
            pltpu.VMEM((128, 128), BF16),
            pltpu.VMEM((2, 2, 384, 128), BF16),
            pltpu.VMEM((2, 2, 272, 512), BF16),
            pltpu.VMEM((2, 512, 512), BF16),
            pltpu.VMEM((512, 1152), F32),
            pltpu.VMEM((2, 256, 128), F32),
            pltpu.VMEM((2, 512, 1024), BF16),
            pltpu.VMEM((2, 512, 512), F32),
            pltpu.VMEM((512, 512), BF16),
            pltpu.VMEM((32, 256, 128), BF16),
            pltpu.VMEM((32, 256, 128), BF16),
            pltpu.VMEM((32, 256, 128), BF16),
            pltpu.VMEM((2, 128, 128), BF16),
            pltpu.VMEM((2, 16, 512), BF16),
            dma((8,)),
            dma((N_COPIES,)),
            dma((N_COPIES,)),
            dma((32,)),
            dma((32,)),
            dma((32,)),
            dma((2, 2, 2)),
            dma((2, 2, 2)),
            dma((2, 2)),
            dma((2, 2)),
        ],
        compiler_params=pltpu.CompilerParams(
            collective_id=0, has_side_effects=True, vmem_limit_bytes=66_000_000
        ),
        name="mixer",
    )(
        tokens, w_pool_in, w_query, w_key.T, w_value.T, w_out, pool_map.reshape(512, 512),
        pool_scale.reshape(1, 512), sinks.reshape(1, 8), q_gain.reshape(1, 64),
        k_gain.reshape(1, 64), norm_gain.reshape(1, 4096),
    )


def solution(mesh):
    in_specs = (
        P("sp", "tp"), P(), P("sp", "tp"), P("sp", "tp"), P("sp", "tp"), P("sp", "tp"),
        P("tp", None, None), P("tp"), P(), P(), P("tp"), P("tp", "sp"),
    )
    out_specs = P(("sp", "tp"), None)
    return jax.shard_map(local_program, mesh=mesh, in_specs=in_specs, out_specs=out_specs, check_vma=False)
```

time: 172 us -> 124 us (0.72)
  the two profiles are of different devices: /device:TPU:1 before, /device:TPU:8 now
where the time goes in v2:
time: 124 us
  Pallas kernels  121 us (98%)
  local copies, waits for them, and re-layouts  3.13 us (3%)
    pallas_call x1, Pallas kernels, local_program(): pl.pallas_call(kernel, out_shape=jax.ShapeDtypeStruct((256, 4096), BF16),...  121 us
    unnamed x1, local copies, waits for them, and re-layouts  3.13 us

profile of v2, /device:TPU:8, one launch (start us, length us, event | category | flops | bytes accessed | tf_op | source)
XLA Modules:
  0.0 123.8 jit_solution(17300618532298069005)
XLA Ops:
  0.0 120.6 %mixer.1 = bf16[256,4096]{1,0:T(8,128)(2,1)} custom-call(bf16[1024,1024]{1,0:T(8,128)(2,1)} %tokens.1, bf16[128,512]{1,0:T(8,128)(2,1)} %wp.1, bf16[128,512]{1,0:T(8,128)(2,1)} %wq.1, bf16[64,128]{1,0:T(8,128)(2,1)} %bitcast.9, bf16[64,128]{1,0:T(8,128)(2,1)} %bitcast.10, bf16[1024,128]{1,0:T(8,128)(2,1)} %wo.1, bf16[512,512]{1,0:T(8,128)(2,1)} %bitcast.8, ...), custom_call_target="tpu_custom_call" | custom-call | tf_op jit(solution)/shard_map/mixer/pallas_call | solution.py:656
  120.6 3.1 %copy.14 = bf16[256,4096]{1,0:T(8,128)(2,1)} copy(bf16[256,4096]{1,0:T(8,128)(2,1)} %mixer.1) | data formatting | bytes 4194304

commit v3 on v2

--- a/solution.py
+++ b/solution.py
@@ -9,7 +9,7 @@
 F32 = jnp.float32
 BF16 = jnp.bfloat16
 EPS = 1e-6
-N_COPIES = 128
+N_GROUPS = 41
 
 
 def mod4(v):
@@ -51,21 +51,25 @@
     cs, ss_, sf_ = 1 - c, f, s
     ssu, ssd, ss2 = mod4(ss_ + 1), mod4(ss_ + 3), mod4(ss_ + 2)
 
-    pending = []
-
-    def send(src, dst, dev):
-        k = len(pending)
-        d = pltpu.make_async_remote_copy(
-            src_ref=src, dst_ref=dst, send_sem=ssem.at[k], recv_sem=rsem.at[k],
+    groups = []
+    W1_SENT, W2_SENT, TOK_SENT, TF_SENT, OTHER_SENT = range(5)
+
+    def group(whole):
+        groups.append(whole)
+        return len(groups) - 1
+
+    def send(src, dst, dev, to, sent):
+        pltpu.make_async_remote_copy(
+            src_ref=src, dst_ref=dst, send_sem=ssem.at[sent], recv_sem=rsem.at[to],
             device_id=dev, device_id_type=MESH,
-        )
-        d.start()
-        pending.append(d)
-        return d
-
-    def recv(*ds):
-        for d in ds:
-            d.wait_recv()
+        ).start()
+
+    def wait(whole, sem):
+        pltpu.make_async_copy(whole, whole, sem).wait()
+
+    def recv(*gs):
+        for g in gs:
+            wait(groups[g], rsem.at[g])
 
     loc = []
 
@@ -166,70 +170,92 @@
     l0.wait()
     l1.wait()
     l3.wait()
-    def halves(src, dst, dev, first):
-        return [
-            send(src.at[pl.ds(r, 64)], dst.at[pl.ds(r, 64)], dev) for r in (first, 64 - first)
-        ]
+    shard1, shard2 = W1.at[0, 0, 0, 0], W2.at[0, 0, 0]
+
+    def send1(piece, dev, to):
+        send(piece, piece, dev, to, W1_SENT)
+
+    def send2(piece, dev, to):
+        send(piece, piece, dev, to, W2_SENT)
 
     def step_a1(g):
         piece = W1.at[g, c, s, f]
-        up, down = halves(piece, piece, dev_fu, 0), halves(piece, piece, dev_fd, 64)
-        return [up[0], down[0]], [up[1], down[1]]
+        to = group(shard1), group(shard1)
+        for k in range(2):
+            send1(piece.at[pl.ds(64 * k, 64)], dev_fu, to[k])
+            send1(piece.at[pl.ds(64 - 64 * k, 64)], dev_fd, to[k])
+        return to
 
     def step_b1(g, a):
-        recv(*a[0])
-        lo, hi = W1.at[g, c, s, fd, pl.ds(0, 64)], W1.at[g, c, s, fu, pl.ds(64, 64)]
-        return [send(lo, lo, dev_fu), send(hi, hi, dev_fd)]
-
-    def step_c1(g, a, b):
-        recv(*a[1], *b)
+        recv(a[0])
+        to = group(shard1)
+        send1(W1.at[g, c, s, fd, pl.ds(0, 64)], dev_fu, to)
+        send1(W1.at[g, c, s, fu, pl.ds(64, 64)], dev_fd, to)
+        return to
+
+    def step_c1(g, a, b, shared):
+        recv(a[1], b)
         plane = W1.at[g, c, s]
-        lo, hi = plane.at[pl.ds(0, 2)], plane.at[pl.ds(2, 2)]
-        first = [send(lo, lo, dev_su), send(hi, hi, dev_sd)]
-        second = [send(hi, hi, dev_su), send(lo, lo, dev_sd)]
-        return first, second, [send(plane, plane, dev_sib)]
+        to = group(W1.at[0, 0, 0]), group(W1.at[0, 0, 0])
+        for k in range(2):
+            send1(plane.at[pl.ds(2 * k, 2)], dev_su, to[k])
+            send1(plane.at[pl.ds(2 - 2 * k, 2)], dev_sd, to[k])
+        send1(plane, dev_sib, shared)
+        return to
 
     def step_d1(g, cc):
-        recv(*cc[0])
-        lo, hi = W1.at[g, c, sd, pl.ds(0, 2)], W1.at[g, c, su, pl.ds(2, 2)]
-        return [send(lo, lo, dev_su), send(hi, hi, dev_sd)]
-
-    def share1(g, s_):
-        piece = W1.at[g, c, s_]
-        return send(piece, piece, dev_sib)
+        recv(cc[0])
+        to = group(W1.at[0, 0, 0])
+        send1(W1.at[g, c, sd, pl.ds(0, 2)], dev_su, to)
+        send1(W1.at[g, c, su, pl.ds(2, 2)], dev_sd, to)
+        return to
+
+    def share1(g, s_, to):
+        send1(W1.at[g, c, s_], dev_sib, to)
 
     def step_a2(g):
-        piece = W2.at[c, s, f, g]
-        return [send(piece, piece, dev_fu), send(piece, piece, dev_fd)]
+        to = group(shard2)
+        for dev in (dev_fu, dev_fd):
+            send2(W2.at[c, s, f, g], dev, to)
+        return to
 
     def step_b2(g, a):
-        recv(*a)
-        lo, hi = W2.at[c, s, fd, g, pl.ds(0, 512)], W2.at[c, s, fu, g, pl.ds(512, 512)]
-        return [send(lo, lo, dev_fu), send(hi, hi, dev_fd)]
-
-    x_w1 = halves(own1, ST1, dev_dx, 0)
+        recv(a)
+        to = group(shard2.at[0])
+        send2(W2.at[c, s, fd, g, pl.ds(0, 512)], dev_fu, to)
+        send2(W2.at[c, s, fu, g, pl.ds(512, 512)], dev_fd, to)
+        return to
+
+    x_w1 = [group(shard1.at[pl.ds(0, 64)]) for _ in range(2)]
+    for k in range(2):
+        part = pl.ds(64 * k, 64)
+        send(own1.at[part], ST1.at[part], dev_dx, x_w1[k], W1_SENT)
     a1 = step_a1(0)
     a2 = step_a2(0)
-    x_w2 = send(W2.at[c, s, f, 0], ST2, dev_dx)
-
-    f_w1 = []
-    b1 = None
+    x_w2 = group(shard2.at[0])
+    send(W2.at[c, s, f, 0], ST2, dev_dx, x_w2, W2_SENT)
+
+    f_w1 = group(shard1)
     for k in range(2):
         recv(x_w1[k])
         part = pl.ds(64 * k, 64)
-        f_w1.append(send(ST1.at[part], W1.at[1, c, s, f, part], dev_dx))
+        send(ST1.at[part], W1.at[1, c, s, f, part], dev_dx, f_w1, W1_SENT)
         if k == 0:
             b1 = step_b1(0, a1)
-    c1a, c1b, sib1 = step_c1(0, a1, b1)
+    sib1 = group(W1.at[0, 0])
+    c1a, c1b = step_c1(0, a1, b1, sib1)
     recv(x_w2)
-    f_w2 = send(ST2, W2.at[c, s, f, 1], dev_dx)
-    tn = [
-        send(tokens.at[pl.ds(n * 256, 256)], TOK.at[0, x], dev_n),
-        send(tokens.at[pl.ds(x2 * 256, 256)], TOK.at[1, x], dev_n),
-    ]
-    sc_c = [send(scale_in, SCALE, dev_x2), send(sinks_in, SINK, dev_x2)]
-
-    recv(*f_w1)
+    f_w2 = group(shard2.at[0])
+    send(ST2, W2.at[c, s, f, 1], dev_dx, f_w2, W2_SENT)
+    two_slabs = TOK.at[0, pl.ds(0, 2)]
+    tn = group(two_slabs)
+    send(tokens.at[pl.ds(n * 256, 256)], TOK.at[0, x], dev_n, tn, TOK_SENT)
+    send(tokens.at[pl.ds(x2 * 256, 256)], TOK.at[1, x], dev_n, tn, TOK_SENT)
+    sc_c, sk_c = group(SCALE), group(SINK)
+    send(scale_in, SCALE, dev_x2, sc_c, OTHER_SENT)
+    send(sinks_in, SINK, dev_x2, sk_c, OTHER_SENT + 1)
+
+    recv(f_w1)
     a1o = step_a1(1)
 
     def scale_slab(j):
@@ -256,29 +282,32 @@
     a2o = step_a2(1)
     b2 = step_b2(0, a2)
     d1 = step_d1(0, (c1a, c1b))
-    c1oa, c1ob, sib1o = step_c1(1, a1o, b1o)
-    tp_ = [
-        send(tokens.at[pl.ds(p * 256, 256)], TOK.at[0, x], dev_p),
-        send(tokens.at[pl.ds(x * 256, 256)], TOK.at[1, x], dev_p),
-    ]
-    recv(*c1b)
-    sib1 += [share1(0, sd), share1(0, su)]
-    recv(*tn)
-    tf = [
-        send(TOK.at[0, n], TOK.at[1, n], dev_p),
-        send(TOK.at[1, n], TOK.at[0, n], dev_p),
-    ]
+    sib1o = group(W1.at[0, 0, pl.ds(0, 3)])
+    c1o = step_c1(1, a1o, b1o, sib1o)
+    tp_ = group(two_slabs)
+    send(tokens.at[pl.ds(p * 256, 256)], TOK.at[0, x], dev_p, tp_, TOK_SENT)
+    send(tokens.at[pl.ds(x * 256, 256)], TOK.at[1, x], dev_p, tp_, TOK_SENT)
+    recv(c1b)
+    share1(0, sd, sib1)
+    share1(0, su, sib1)
+    recv(tn)
+    tf = group(two_slabs)
+    send(TOK.at[0, n], TOK.at[1, n], dev_p, tf, TF_SENT)
+    send(TOK.at[1, n], TOK.at[0, n], dev_p, tf, TF_SENT)
     l6.wait()
     half = pl.ds(c * 256, 256)
-    x_pm = send(PM.at[0, half], ST3, dev_dx)
+    x_pm = group(ST3)
+    send(PM.at[0, half], ST3, dev_dx, x_pm, OTHER_SENT + 2)
     b2o = step_b2(1, a2o)
 
     def half_plane(s_, k):
         return W2.at[c, s_, pl.ds(2 * k, 2)]
 
     def c2_send(k_up, k_dn):
-        u, d = half_plane(s, k_up), half_plane(s, k_dn)
-        return [send(u, u, dev_su), send(d, d, dev_sd)]
+        to = group(W2.at[0, 0])
+        send2(half_plane(s, k_up), dev_su, to)
+        send2(half_plane(s, k_dn), dev_sd, to)
+        return to
 
     def matmul(gi, jz):
         parts = []
@@ -499,54 +528,66 @@
 
         lax.fori_loop(0, 2, body, 0)
 
-    recv(*d1)
-    sib1.append(share1(0, s2))
+    recv(d1)
+    share1(0, s2, sib1)
     ACC[...] = jnp.zeros_like(ACC)
-    recv(*sib1)
+    recv(sib1)
     matmul_slab(0, x)
-    recv(*tp_)
+    recv(tp_)
     scale_slab(p)
     matmul_slab(0, p)
-    d1o = step_d1(1, (c1oa, c1ob))
-    recv(*b2, *b2o)
+    d1o = step_d1(1, c1o)
+    recv(b2, b2o)
     c2a = c2_send(0, 1)
     c2b = c2_send(1, 0)
-    plane2 = W2.at[c, s]
-    sib2_own = [send(plane2, plane2, dev_sib)]
-    for d in tf:
-        d.wait_send()
+    sib2_own = group(W2.at[0, 0])
+    send2(W2.at[c, s], dev_sib, sib2_own)
+    wait(two_slabs, ssem.at[TF_SENT])
     scale_slab(n)
     matmul_slab(0, n)
-    recv(*tf)
+    recv(tf)
     scale_slab(x2)
     matmul_slab(0, x2)
     post(0)
     halo_send(0)
-    recv(*c1ob)
-    sib1o += [share1(1, sd), share1(1, su)]
+    recv(c1o[1])
+    share1(1, sd, sib1o)
+    share1(1, su, sib1o)
     recv(x_pm)
-    f_pm = send(ST3, PM.at[1, half], dev_dx)
+    f_pm = group(ST3)
+    send(ST3, PM.at[1, half], dev_dx, f_pm, OTHER_SENT + 3)
     ACC[...] = jnp.zeros_like(ACC)
     matmul_planes(1, c, s, s, 1)
     matmul_planes(1, c, sd, su, 2)
-    recv(*sib1o)
+    recv(sib1o)
     matmul_planes(1, cs, ss_, ss_, 1)
     matmul_planes(1, cs, ssd, ssu, 2)
     halo_relay(0)
     attend(0, 1)
-    recv(*d1o)
-    sib1o_far = share1(1, s2)
+    recv(d1o)
+    sib1o_far = group(W1.at[0, 0, 0])
+    share1(1, s2, sib1o_far)
     matmul_planes(1, c, s2, s2, 1)
     recv(sib1o_far)
     matmul_planes(1, cs, ss2, ss2, 1)
     post(1)
     halo_send(1)
 
-    recv(*sc_c)
+    recv(sc_c, sk_c)
     attend(1, 1)
     halo_relay(1)
     recv(f_pm)
-    sib_pm = send(PM.at[1, half], PM.at[1, half], dev_sib)
+    sib_pm = group(ST3)
+    send(PM.at[1, half], PM.at[1, half], dev_sib, sib_pm, OTHER_SENT + 4)
+    recv(c2a)
+    u0, d0 = half_plane(sd, 0), half_plane(su, 1)
+    d2 = [group(W2.at[0, 0, pl.ds(0, 2)]) for _ in range(2)]
+    for k in range(2):
+        send2(u0.at[k], dev_su, d2[k])
+        send2(d0.at[k], dev_sd, d2[k])
+    sib2_a = group(W2.at[0, 0])
+    send2(u0, dev_sib, sib2_a)
+    send2(d0, dev_sib, sib2_a)
     halo_wait(0)
     attend(0, 0)
     pool(0, x)
@@ -554,10 +595,6 @@
     attend(1, 0)
     recv(sib_pm)
     pool(1, x2)
-    recv(*c2a)
-    u0, d0 = half_plane(sd, 0), half_plane(su, 1)
-    d2 = [[send(u0.at[k], u0.at[k], dev_su), send(d0.at[k], d0.at[k], dev_sd)] for k in range(2)]
-    sib2_a = [send(u0, u0, dev_sib), send(d0, d0, dev_sib)]
 
     def unit(u, cc, s_, fs):
         rhs = []
@@ -570,21 +607,18 @@
             idx = 2 * u + e
             OWNB[idx] = ob[0:256, e * 128 : (e + 1) * 128]
             SENDB[idx] = ob[256:512, e * 128 : (e + 1) * 128]
-            out_copy(idx).start()
-
-    def out_copy(idx):
-        return pltpu.make_async_remote_copy(
-            src_ref=SENDB.at[idx], dst_ref=RECVB.at[idx], send_sem=osend.at[idx],
-            recv_sem=orecv.at[idx], device_id=dev_p, device_id_type=MESH,
-        )
+            pltpu.make_async_remote_copy(
+                src_ref=SENDB.at[idx], dst_ref=RECVB.at[idx], send_sem=osend, recv_sem=orecv.at[u],
+                device_id=dev_p, device_id_type=MESH,
+            ).start()
 
     def total(u, cc, s_, fs):
+        wait(RECVB.at[pl.ds(2 * u, 2)], orecv.at[u])
         for e in range(2):
             idx = 2 * u + e
             col = pl.ds(pl.multiple_of(sp_of(cc, fs[e], s_) * 128, 128), 128)
-            out_copy(idx).wait_recv()
             OWNB[idx] = (OWNB[idx].astype(F32) + RECVB[idx].astype(F32)).astype(BF16)
-            pltpu.make_async_copy(OWNB.at[idx], out.at[:, col], oloc.at[idx]).start()
+            pltpu.make_async_copy(OWNB.at[idx], out.at[:, col], oloc).start()
 
     def pair(stage, mine, sA, kA, sB, kB, act=unit):
         cc = c if mine else cs
@@ -596,54 +630,57 @@
 
         lax.fori_loop(0, 2, body, 0)
 
+    def far_unit(u, cc, s_, k, act):
+        def body(t, carry):
+            act(u, cc, s_, (t, 2 + t))
+            return carry
+
+        lax.fori_loop(k, k + 1, body, 0)
+
     pair(0, True, s, 0, s, 1)
-    recv(*sib2_own)
+    recv(sib2_own)
     pair(0, False, ss_, 0, ss_, 1)
-
     pair(1, True, sd, 0, su, 1)
-    recv(*sib2_a)
+    recv(c2b)
+    sib2_b = group(W2.at[0, 0])
+    send2(half_plane(sd, 1), dev_sib, sib2_b)
+    send2(half_plane(su, 0), dev_sib, sib2_b)
+    recv(sib2_a)
     pair(1, False, ssd, 0, ssu, 1)
-    recv(*c2b)
-    u1, d1_ = half_plane(sd, 1), half_plane(su, 0)
-    sib2_b = [send(u1, u1, dev_sib), send(d1_, d1_, dev_sib)]
     pair(2, True, sd, 1, su, 0)
-    recv(*sib2_b)
-    pair(2, False, ssd, 1, ssu, 0)
-
     pair(0, True, s, 0, s, 1, total)
     pair(0, False, ss_, 0, ss_, 1, total)
+    recv(sib2_b)
+    pair(2, False, ssd, 1, ssu, 0)
+
     for k in range(2):
-        recv(*d2[k])
-        far = [W2.at[c, s2, k], W2.at[c, s2, 2 + k]]
-        sib2_c = [send(r, r, dev_sib) for r in far]
-        unit(12 + 2 * k, c, s2, (k, 2 + k))
-        recv(*sib2_c)
-        unit(13 + 2 * k, cs, ss2, (k, 2 + k))
+        recv(d2[k])
+        sib2_c = group(W2.at[0, 0, pl.ds(0, 2)])
+        send2(W2.at[c, s2, k], dev_sib, sib2_c)
+        send2(W2.at[c, s2, 2 + k], dev_sib, sib2_c)
+        far_unit(12 + 2 * k, c, s2, k, unit)
+        recv(sib2_c)
+        far_unit(13 + 2 * k, cs, ss2, k, unit)
         if k == 0:
             pair(1, True, sd, 0, su, 1, total)
             pair(1, False, ssd, 0, ssu, 1, total)
-
-    pair(2, True, sd, 1, su, 0, total)
-    pair(2, False, ssd, 1, ssu, 0, total)
-    for k in range(2):
-        total(12 + 2 * k, c, s2, (k, 2 + k))
-        total(13 + 2 * k, cs, ss2, (k, 2 + k))
-
-    tf_ids = {id(d) for d in tf}
-    for d in pending:
-        if id(d) not in tf_ids:
-            d.wait_send()
+            pair(2, True, sd, 1, su, 0, total)
+            pair(2, False, ssd, 1, ssu, 0, total)
+
+    wait(W1, ssem.at[W1_SENT])
+    wait(W2, ssem.at[W2_SENT])
+    wait(TOK.at[0], ssem.at[TOK_SENT])
+    for k, whole in enumerate((SCALE, SINK, ST3, ST3, ST3)):
+        wait(whole, ssem.at[OTHER_SENT + k])
     for gi in range(2):
         halo_sent(gi)
         relay_sent(gi)
-
-    def drain(idx, carry):
-        out_copy(idx).wait_send()
-        col = pl.ds(pl.multiple_of(idx * 128, 128), 128)
-        pltpu.make_async_copy(OWNB.at[idx], out.at[:, col], oloc.at[idx]).wait()
-        return carry
-
-    lax.fori_loop(0, 32, drain, 0)
+    wait(SENDB, osend)
+    for k in range(2):
+        far_unit(12 + 2 * k, c, s2, k, total)
+        far_unit(13 + 2 * k, cs, ss2, k, total)
+    wait(OWNB, oloc)
+    assert len(groups) == N_GROUPS, len(groups)
 
 
 def local_program(
@@ -683,11 +720,11 @@
             pltpu.VMEM((2, 128, 128), BF16),
             pltpu.VMEM((2, 16, 512), BF16),
             dma((8,)),
-            dma((N_COPIES,)),
-            dma((N_COPIES,)),
-            dma((32,)),
-            dma((32,)),
-            dma((32,)),
+            dma((9,)),
+            dma((N_GROUPS,)),
+            dma(()),
+            dma((16,)),
+            dma(()),
             dma((2, 2, 2)),
             dma((2, 2, 2)),
             dma((2, 2)),

time: 124 us -> 122 us (0.984)
  the two profiles are of different devices: /device:TPU:8 before, /device:TPU:1 now
where the time goes in v3:
time: 122 us
  Pallas kernels  118 us (97%)
  local copies, waits for them, and re-layouts  3.13 us (3%)
    pallas_call x1, Pallas kernels, local_program(): pl.pallas_call(kernel, out_shape=jax.ShapeDtypeStruct((256, 4096), BF16),...  118 us
    unnamed x1, local copies, waits for them, and re-layouts  3.13 us

profile of v3, /device:TPU:1, one launch (start us, length us, event | category | flops | bytes accessed | tf_op | source)
XLA Modules:
  0.0 121.6 jit_solution(3316775186521013463)
XLA Ops:
  0.0 118.4 %mixer.1 = bf16[256,4096]{1,0:T(8,128)(2,1)} custom-call(bf16[1024,1024]{1,0:T(8,128)(2,1)} %tokens.1, bf16[128,512]{1,0:T(8,128)(2,1)} %wp.1, bf16[128,512]{1,0:T(8,128)(2,1)} %wq.1, bf16[64,128]{1,0:T(8,128)(2,1)} %bitcast.9, bf16[64,128]{1,0:T(8,128)(2,1)} %bitcast.10, bf16[1024,128]{1,0:T(8,128)(2,1)} %wo.1, bf16[512,512]{1,0:T(8,128)(2,1)} %bitcast.8, ...), custom_call_target="tpu_custom_call" | custom-call | tf_op jit(solution)/shard_map/mixer/pallas_call | solution.py:693
  118.4 3.1 %copy.14 = bf16[256,4096]{1,0:T(8,128)(2,1)} copy(bf16[256,4096]{1,0:T(8,128)(2,1)} %mixer.1) | data formatting | bytes 4194304

commit v4 on v3

--- a/solution.py
+++ b/solution.py
@@ -232,9 +232,6 @@
         send(own1.at[part], ST1.at[part], dev_dx, x_w1[k], W1_SENT)
     a1 = step_a1(0)
     a2 = step_a2(0)
-    x_w2 = group(shard2.at[0])
-    send(W2.at[c, s, f, 0], ST2, dev_dx, x_w2, W2_SENT)
-
     f_w1 = group(shard1)
     for k in range(2):
         recv(x_w1[k])
@@ -242,11 +239,6 @@
         send(ST1.at[part], W1.at[1, c, s, f, part], dev_dx, f_w1, W1_SENT)
         if k == 0:
             b1 = step_b1(0, a1)
-    sib1 = group(W1.at[0, 0])
-    c1a, c1b = step_c1(0, a1, b1, sib1)
-    recv(x_w2)
-    f_w2 = group(shard2.at[0])
-    send(ST2, W2.at[c, s, f, 1], dev_dx, f_w2, W2_SENT)
     two_slabs = TOK.at[0, pl.ds(0, 2)]
     tn = group(two_slabs)
     send(tokens.at[pl.ds(n * 256, 256)], TOK.at[0, x], dev_n, tn, TOK_SENT)
@@ -255,6 +247,9 @@
     send(scale_in, SCALE, dev_x2, sc_c, OTHER_SENT)
     send(sinks_in, SINK, dev_x2, sk_c, OTHER_SENT + 1)
 
+    b2 = step_b2(0, a2)
+    sib1 = group(W1.at[0, 0])
+    c1a, c1b = step_c1(0, a1, b1, sib1)
     recv(f_w1)
     a1o = step_a1(1)
 
@@ -278,63 +273,60 @@
     l5.wait()
     scale_slab(x)
     b1o = step_b1(1, a1o)
-    recv(f_w2)
-    a2o = step_a2(1)
-    b2 = step_b2(0, a2)
-    d1 = step_d1(0, (c1a, c1b))
-    sib1o = group(W1.at[0, 0, pl.ds(0, 3)])
-    c1o = step_c1(1, a1o, b1o, sib1o)
     tp_ = group(two_slabs)
     send(tokens.at[pl.ds(p * 256, 256)], TOK.at[0, x], dev_p, tp_, TOK_SENT)
     send(tokens.at[pl.ds(x * 256, 256)], TOK.at[1, x], dev_p, tp_, TOK_SENT)
-    recv(c1b)
-    share1(0, sd, sib1)
-    share1(0, su, sib1)
     recv(tn)
     tf = group(two_slabs)
     send(TOK.at[0, n], TOK.at[1, n], dev_p, tf, TF_SENT)
     send(TOK.at[1, n], TOK.at[0, n], dev_p, tf, TF_SENT)
-    l6.wait()
-    half = pl.ds(c * 256, 256)
-    x_pm = group(ST3)
-    send(PM.at[0, half], ST3, dev_dx, x_pm, OTHER_SENT + 2)
-    b2o = step_b2(1, a2o)
+    d1 = step_d1(0, (c1a, c1b))
+    sib1o = group(W1.at[0, 0, pl.ds(0, 3)])
+    c1o = step_c1(1, a1o, b1o, sib1o)
+    recv(c1b)
+    share1(0, sd, sib1)
+    share1(0, su, sib1)
 
     def half_plane(s_, k):
         return W2.at[c, s_, pl.ds(2 * k, 2)]
 
-    def c2_send(k_up, k_dn):
-        to = group(W2.at[0, 0])
-        send2(half_plane(s, k_up), dev_su, to)
-        send2(half_plane(s, k_dn), dev_sd, to)
-        return to
-
-    def matmul(gi, jz):
-        parts = []
-        for yy in range(4):
-            parts.append(W1[gi, 0, jz, yy])
-            parts.append(W1[gi, 1, yy, jz])
-        rhs = jnp.concatenate(parts, axis=0)
-        lhs = TOK[:, jz].reshape(512, 1024)
-        ACC[...] += jnp.dot(lhs, rhs, preferred_element_type=F32)
-
-    def matmul_slab(gi, jz):
-        lax.fori_loop(0, 1, lambda t, carry: (matmul(gi, jz), carry)[1], 0)
-
-    def matmul_planes(gi, cc, sA, sB, count):
+    def c2_send(g):
+        to = c2a, c2b
+        for k in range(2):
+            send2(W2.at[c, s, pl.ds(2 * k, 2), g], dev_su, to[k])
+            send2(W2.at[c, s, pl.ds(2 - 2 * k, 2), g], dev_sd, to[k])
+
+    def matmul(lhs, rhs, first):
+        o = jnp.dot(lhs, rhs, preferred_element_type=F32)
+        if first:
+            ACC[...] = o
+        else:
+            ACC[...] += o
+
+    def matmul_slab(gi, jz, first=False):
         def body(t, carry):
-            s_ = sA + t * (sB - sA)
-            rhs = jnp.concatenate([W1[gi, cc, s_, k] for k in range(4)], axis=0)
-            lhs = []
-            for k in range(4):
-                off = ((1 - cc) * k + cc * s_) * 256 + cc * 128
-                col = pl.ds(pl.multiple_of(off, 128), 128)
-                lhs.append(TOK[:, (1 - cc) * s_ + cc * k, :, col].reshape(512, 128))
-            lhs = jnp.concatenate(lhs, axis=1)
-            ACC[...] += jnp.dot(lhs, rhs, preferred_element_type=F32)
+            parts = []
+            for yy in range(4):
+                parts.append(W1[gi, 0, jz, yy])
+                parts.append(W1[gi, 1, yy, jz])
+            matmul(TOK[:, jz].reshape(512, 1024), jnp.concatenate(parts, axis=0), first)
             return carry
 
-        lax.fori_loop(0, count, body, 0)
+        lax.fori_loop(0, 1, body, 0)
+
+    def matmul_planes(gi, cc, planes, first=False):
+        def body(t, carry):
+            lhs, rhs = [], []
+            for s_ in planes:
+                for k in range(4):
+                    rhs.append(W1[gi, cc, s_, k])
+                    off = ((1 - cc) * k + cc * s_) * 256 + cc * 128
+                    col = pl.ds(pl.multiple_of(off, 128), 128)
+                    lhs.append(TOK[:, (1 - cc) * s_ + cc * k, :, col].reshape(512, 128))
+            matmul(jnp.concatenate(lhs, axis=1), jnp.concatenate(rhs, axis=0), first)
+            return carry
+
+        lax.fori_loop(0, 1, body, 0)
 
     def post(gi):
         def body(k, carry):
@@ -530,18 +522,21 @@
 
     recv(d1)
     share1(0, s2, sib1)
-    ACC[...] = jnp.zeros_like(ACC)
     recv(sib1)
-    matmul_slab(0, x)
+    matmul_slab(0, x, True)
     recv(tp_)
     scale_slab(p)
     matmul_slab(0, p)
     d1o = step_d1(1, c1o)
-    recv(b2, b2o)
-    c2a = c2_send(0, 1)
-    c2b = c2_send(1, 0)
-    sib2_own = group(W2.at[0, 0])
-    send2(W2.at[c, s], dev_sib, sib2_own)
+    c2a, c2b = group(W2.at[0, 0]), group(W2.at[0, 0])
+    recv(b2)
+    c2_send(0)
+    x_w2 = group(shard2.at[0])
+    send(W2.at[c, s, f, 0], ST2, dev_dx, x_w2, W2_SENT)
+    l6.wait()
+    half = pl.ds(c * 256, 256)
+    x_pm = group(ST3)
+    send(PM.at[0, half], ST3, dev_dx, x_pm, OTHER_SENT + 2)
     wait(two_slabs, ssem.at[TF_SENT])
     scale_slab(n)
     matmul_slab(0, n)
@@ -553,23 +548,26 @@
     recv(c1o[1])
     share1(1, sd, sib1o)
     share1(1, su, sib1o)
+    recv(x_w2)
+    f_w2 = group(shard2.at[0])
+    send(ST2, W2.at[c, s, f, 1], dev_dx, f_w2, W2_SENT)
+    matmul_planes(1, c, (s, sd, su), True)
+    recv(sib1o)
+    recv(f_w2)
+    a2o = step_a2(1)
     recv(x_pm)
     f_pm = group(ST3)
     send(ST3, PM.at[1, half], dev_dx, f_pm, OTHER_SENT + 3)
-    ACC[...] = jnp.zeros_like(ACC)
-    matmul_planes(1, c, s, s, 1)
-    matmul_planes(1, c, sd, su, 2)
-    recv(sib1o)
-    matmul_planes(1, cs, ss_, ss_, 1)
-    matmul_planes(1, cs, ssd, ssu, 2)
+    matmul_planes(1, cs, (ss_, ssd, ssu))
     halo_relay(0)
     attend(0, 1)
     recv(d1o)
     sib1o_far = group(W1.at[0, 0, 0])
     share1(1, s2, sib1o_far)
-    matmul_planes(1, c, s2, s2, 1)
+    matmul_planes(1, c, (s2,))
     recv(sib1o_far)
-    matmul_planes(1, cs, ss2, ss2, 1)
+    matmul_planes(1, cs, (ss2,))
+    b2o = step_b2(1, a2o)
     post(1)
     halo_send(1)
 
@@ -579,15 +577,10 @@
     recv(f_pm)
     sib_pm = group(ST3)
     send(PM.at[1, half], PM.at[1, half], dev_sib, sib_pm, OTHER_SENT + 4)
-    recv(c2a)
-    u0, d0 = half_plane(sd, 0), half_plane(su, 1)
-    d2 = [group(W2.at[0, 0, pl.ds(0, 2)]) for _ in range(2)]
-    for k in range(2):
-        send2(u0.at[k], dev_su, d2[k])
-        send2(d0.at[k], dev_sd, d2[k])
-    sib2_a = group(W2.at[0, 0])
-    send2(u0, dev_sib, sib2_a)
-    send2(d0, dev_sib, sib2_a)
+    recv(b2o)
+    c2_send(1)
+    sib2_own = group(W2.at[0, 0])
+    send2(W2.at[c, s], dev_sib, sib2_own)
     halo_wait(0)
     attend(0, 0)
     pool(0, x)
@@ -640,13 +633,22 @@
     pair(0, True, s, 0, s, 1)
     recv(sib2_own)
     pair(0, False, ss_, 0, ss_, 1)
+    recv(c2a)
+    u0, d0 = half_plane(sd, 0), half_plane(su, 1)
+    d2 = [group(W2.at[0, 0, pl.ds(0, 2)]) for _ in range(2)]
+    for k in range(2):
+        send2(u0.at[k], dev_su, d2[k])
+        send2(d0.at[k], dev_sd, d2[k])
+    sib2_a = group(W2.at[0, 0])
+    send2(u0, dev_sib, sib2_a)
+    send2(d0, dev_sib, sib2_a)
     pair(1, True, sd, 0, su, 1)
+    recv(sib2_a)
+    pair(1, False, ssd, 0, ssu, 1)
     recv(c2b)
     sib2_b = group(W2.at[0, 0])
     send2(half_plane(sd, 1), dev_sib, sib2_b)
     send2(half_plane(su, 0), dev_sib, sib2_b)
-    recv(sib2_a)
-    pair(1, False, ssd, 0, ssu, 1)
     pair(2, True, sd, 1, su, 0)
     pair(0, True, s, 0, s, 1, total)
     pair(0, False, ss_, 0, ss_, 1, total)
@@ -664,8 +666,6 @@
         if k == 0:
             pair(1, True, sd, 0, su, 1, total)
             pair(1, False, ssd, 0, ssu, 1, total)
-            pair(2, True, sd, 1, su, 0, total)
-            pair(2, False, ssd, 1, ssu, 0, total)
 
     wait(W1, ssem.at[W1_SENT])
     wait(W2, ssem.at[W2_SENT])
@@ -676,6 +676,8 @@
         halo_sent(gi)
         relay_sent(gi)
     wait(SENDB, osend)
+    pair(2, True, sd, 1, su, 0, total)
+    pair(2, False, ssd, 1, ssu, 0, total)
     for k in range(2):
         far_unit(12 + 2 * k, c, s2, k, total)
         far_unit(13 + 2 * k, cs, ss2, k, total)

time: 122 us -> 117 us (0.959)
  Pallas kernels: 118 us -> 114 us
    pallas_call x1, Pallas kernels: 118 us -> 114 us  [local_program(): pl.pallas_call(kernel, out_shape=jax.ShapeDtypeStruct((256, 4096), BF16),...]
where the time goes in v4:
time: 117 us
  Pallas kernels  114 us (97%)
  local copies, waits for them, and re-layouts  3.13 us (3%)
    pallas_call x1, Pallas kernels, local_program(): pl.pallas_call(kernel, out_shape=jax.ShapeDtypeStruct((256, 4096), BF16),...  114 us
    unnamed x1, local copies, waits for them, and re-layouts  3.13 us

profile of v4, /device:TPU:1, one launch (start us, length us, event | category | flops | bytes accessed | tf_op | source)
XLA Modules:
  0.0 117.0 jit_solution(2007662208224229429)
XLA Ops:
  0.0 113.8 %mixer.1 = bf16[256,4096]{1,0:T(8,128)(2,1)} custom-call(bf16[1024,1024]{1,0:T(8,128)(2,1)} %tokens.1, bf16[128,512]{1,0:T(8,128)(2,1)} %wp.1, bf16[128,512]{1,0:T(8,128)(2,1)} %wq.1, bf16[64,128]{1,0:T(8,128)(2,1)} %bitcast.9, bf16[64,128]{1,0:T(8,128)(2,1)} %bitcast.10, bf16[1024,128]{1,0:T(8,128)(2,1)} %wo.1, bf16[512,512]{1,0:T(8,128)(2,1)} %bitcast.8, ...), custom_call_target="tpu_custom_call" | custom-call | tf_op jit(solution)/shard_map/mixer/pallas_call | solution.py:695
  113.8 3.1 %copy.14 = bf16[256,4096]{1,0:T(8,128)(2,1)} copy(bf16[256,4096]{1,0:T(8,128)(2,1)} %mixer.1) | data formatting | bytes 4194304

commit v5 on v4

--- a/solution.py
+++ b/solution.py
@@ -9,7 +9,8 @@
 F32 = jnp.float32
 BF16 = jnp.bfloat16
 EPS = 1e-6
-N_GROUPS = 41
+N_GROUPS = 43
+PIECES = 8
 
 
 def mod4(v):
@@ -17,9 +18,9 @@
 
 
 def kernel(
-    tokens, wp, wq, wk_t, wv_t, wo, pmap, scale_in, sinks_in, q_gain, k_gain, gain,
+    tokens, wp, wq, wk_t, wv_t, wo, pmap, scale_in, sinks_in, q_in, k_in, gain_in,
     out,
-    W1, W2, TOK, ST1, ST2, ST3, PM, SCALE, SINK, KVT, KV, PB, QB, ACC, SS, MIX, BIAS, BLK, SENDB, OWNB, RECVB, RLK, RLP,
+    W1, W2, TOK, ST1, ST2, ST3, PM, SCALE, SINK, q_gain, k_gain, gain, KVT, KV, PB, QB, ACC, SS, MIX, BIAS, BLK, SENDB, OWNB, RECVB, RLK, RLP,
     lsem, ssem, rsem, osend, orecv, oloc, hsend, hrecv, rlsend, rlrecv,
 ):
     sp = lax.axis_index("sp")
@@ -71,6 +72,62 @@
         for g in gs:
             wait(groups[g], rsem.at[g])
 
+    def holder(q, c_):
+        inner = lax.rem(lax.div(q + 1, 2), 2)
+        even = lax.div(q, 2) * 2 + par
+        odd = inner * (2 - par) + (1 - inner) * 3 * par
+        return (1 - c_) * even + c_ * odd
+
+    quarters = (x, p)
+
+    def halo_to(i):
+        q = quarters[i]
+        qn = mod4(q + 1)
+        spn = sp + lax.div(q + 1, 4)
+        xn = holder(qn, lax.rem(spn, 2))
+        here = (spn == sp) & (xn == x)
+        away = jnp.logical_not(here) & (spn < 32)
+        passed = away & (c == 1) & (q == 3)
+        return qn, jnp.where(spn < 32, spn, 0), xn, here, away & jnp.logical_not(passed), passed
+
+    def halo_from(i):
+        q = quarters[i]
+        first = (sp == 0) & (q == 0)
+        back = jnp.where(q == 0, 1, 0)
+        relayed = (back == 1) & (c == 0)
+        spp = jnp.where(first, sp, sp - back - jnp.where(relayed, 1, 0))
+        xp = holder(mod4(q + 3), lax.rem(sp - back + 2, 2))
+        here = (back == 0) & (xp == x)
+        return first, jnp.logical_not(first) & jnp.logical_not(here), spp, xp
+
+    relay = (c == 0) & ((x == 0) | (x == 3)) & (sp < 30)
+    relay_dev = (jnp.where(relay, sp + 2, 0), par)
+    relay_slot = jnp.where(par == 0, 0, 1)
+
+    barrier = pltpu.get_barrier_semaphore()
+
+    def greet(dev):
+        pl.semaphore_signal(barrier, inc=1, device_id=dev, device_id_type=MESH)
+
+    for dev in (dev_fu, dev_fd, dev_su, dev_sd, dev_sib, dev_p, dev_n, dev_x2):
+        greet(dev)
+    @pl.when(relay)
+    def _():
+        greet(relay_dev)
+
+    for i in range(2):
+        _, spn, xn, _, away, _ = halo_to(i)
+
+        @pl.when(away)
+        def _():
+            greet((spn, xn))
+
+        _, apart, spp, xp = halo_from(i)
+
+        @pl.when(apart)
+        def _():
+            greet((spp, xp))
+
     loc = []
 
     def local(src, dst):
@@ -88,62 +145,12 @@
     l4 = local(tokens.at[pl.ds(x * 256, 256)], TOK.at[0, x])
     l5 = local(tokens.at[pl.ds(p * 256, 256)], TOK.at[1, x])
     l6 = local(pmap, PM.at[0])
-
-    def holder(q, c_):
-        inner = lax.rem(lax.div(q + 1, 2), 2)
-        even = lax.div(q, 2) * 2 + par
-        odd = inner * (2 - par) + (1 - inner) * 3 * par
-        return (1 - c_) * even + c_ * odd
-
-    quarters = (x, p)
-
-    def halo_to(i):
-        q = quarters[i]
-        qn = mod4(q + 1)
-        spn = sp + lax.div(q + 1, 4)
-        xn = holder(qn, lax.rem(spn, 2))
-        here = (spn == sp) & (xn == x)
-        away = jnp.logical_not(here) & (spn < 32)
-        passed = away & (c == 1) & (q == 3)
-        return qn, jnp.where(spn < 32, spn, 0), xn, here, away & jnp.logical_not(passed), passed
-
-    def halo_from(i):
-        q = quarters[i]
-        first = (sp == 0) & (q == 0)
-        back = jnp.where(q == 0, 1, 0)
-        relayed = (back == 1) & (c == 0)
-        spp = jnp.where(first, sp, sp - back - jnp.where(relayed, 1, 0))
-        xp = holder(mod4(q + 3), lax.rem(sp - back + 2, 2))
-        here = (back == 0) & (xp == x)
-        return first, jnp.logical_not(first) & jnp.logical_not(here), spp, xp
-
-    relay = (c == 0) & ((x == 0) | (x == 3)) & (sp < 30)
-    relay_dev = (jnp.where(relay, sp + 2, 0), par)
-    relay_slot = jnp.where(par == 0, 0, 1)
-
-    barrier = pltpu.get_barrier_semaphore()
-
-    def greet(dev):
-        pl.semaphore_signal(barrier, inc=1, device_id=dev, device_id_type=MESH)
-
-    for dev in (dev_fu, dev_fd, dev_su, dev_sd, dev_sib, dev_p, dev_n, dev_x2):
-        greet(dev)
-    @pl.when(relay)
-    def _():
-        greet(relay_dev)
-
-    for i in range(2):
-        _, spn, xn, _, away, _ = halo_to(i)
-
-        @pl.when(away)
-        def _():
-            greet((spn, xn))
-
-        _, apart, spp, xp = halo_from(i)
-
-        @pl.when(apart)
-        def _():
-            greet((spp, xp))
+    small = [
+        local(src, dst)
+        for src, dst in (
+            (scale_in, SCALE.at[0]), (sinks_in, SINK.at[0]), (q_in, q_gain), (k_in, k_gain), (gain_in, gain),
+        )
+    ]
 
     lane_i = lax.broadcasted_iota(jnp.int32, (512, 512), 1)
     row_i = lax.broadcasted_iota(jnp.int32, (512, 512), 0)
@@ -154,14 +161,6 @@
         lax.shift_right_logical(lane_i, 6) == lax.shift_right_logical(row_i, 6), 1.0, 0.0
     ).astype(BF16)
     SS[...] = jnp.zeros_like(SS)
-    key_i = jnp.bitwise_and(lane_i, 255)
-    dist = 128 + jnp.bitwise_and(row_i, 127) - key_i
-    band = (dist >= 0) & (dist < 128)
-    head_in = 2 * lax.shift_right_logical(row_i, 7) + lax.shift_right_logical(lane_i, 8) + 1
-    for gi, g in ((0, x), (1, x2)):
-        slope = jnp.exp2(-0.25 * (g * 8 + head_in).astype(F32))
-        BIAS[gi] = jnp.where(band, -slope * dist.astype(F32), -1e30)
-
     peers = 8 + jnp.where(relay, 1, 0)
     for i in range(2):
         peers += jnp.where(halo_to(i)[4], 1, 0) + jnp.where(halo_from(i)[1], 1, 0)
@@ -232,6 +231,14 @@
         send(own1.at[part], ST1.at[part], dev_dx, x_w1[k], W1_SENT)
     a1 = step_a1(0)
     a2 = step_a2(0)
+    key_i = jnp.bitwise_and(lane_i, 255)
+    dist = 128 + jnp.bitwise_and(row_i, 127) - key_i
+    band = (dist >= 0) & (dist < 128)
+    head_in = 2 * lax.shift_right_logical(row_i, 7) + lax.shift_right_logical(lane_i, 8) + 1
+    for gi, g in ((0, x), (1, x2)):
+        slope = jnp.exp2(-0.25 * (g * 8 + head_in).astype(F32))
+        BIAS[gi] = jnp.where(band, -slope * dist.astype(F32), -1e30)
+
     f_w1 = group(shard1)
     for k in range(2):
         recv(x_w1[k])
@@ -243,9 +250,9 @@
     tn = group(two_slabs)
     send(tokens.at[pl.ds(n * 256, 256)], TOK.at[0, x], dev_n, tn, TOK_SENT)
     send(tokens.at[pl.ds(x2 * 256, 256)], TOK.at[1, x], dev_n, tn, TOK_SENT)
-    sc_c, sk_c = group(SCALE), group(SINK)
-    send(scale_in, SCALE, dev_x2, sc_c, OTHER_SENT)
-    send(sinks_in, SINK, dev_x2, sk_c, OTHER_SENT + 1)
+    sc_c, sk_c = group(SCALE.at[1]), group(SINK.at[1])
+    send(scale_in, SCALE.at[1], dev_x2, sc_c, OTHER_SENT)
+    send(sinks_in, SINK.at[1], dev_x2, sk_c, OTHER_SENT + 1)
 
     b2 = step_b2(0, a2)
     sib1 = group(W1.at[0, 0])
@@ -269,8 +276,8 @@
 
         lax.fori_loop(0, 8, body, 0)
 
-    l4.wait()
-    l5.wait()
+    for d in (l4, l5, *small):
+        d.wait()
     scale_slab(x)
     b1o = step_b1(1, a1o)
     tp_ = group(two_slabs)
@@ -467,12 +474,12 @@
             count = jnp.minimum(pos + 1, span).astype(F32)
             diff = (run * (1.0 / count) - pf[16:]).astype(BF16)
             m = jnp.dot(diff, PM[gi], preferred_element_type=F32)
-            m = m * (scale_in if gi == 0 else SCALE)[...]
+            m = m * SCALE[gi]
             m = m * lax.rsqrt(jnp.mean(m * m, axis=-1, keepdims=True) + EPS)
             MIX[gi, i * 256 : (i + 1) * 256, 0:512] = m.astype(BF16)
 
     def attend(gi, r):
-        sink = jnp.exp((sinks_in if gi == 0 else SINK)[...])
+        sink = jnp.exp(SINK[gi])
         left = lax.broadcasted_iota(jnp.int32, (1, 128), 1) < 64
         es = jnp.concatenate(
             [
@@ -589,12 +596,20 @@
     recv(sib_pm)
     pool(1, x2)
 
+    def product(cc, s_, fs, g):
+        rhs = jnp.concatenate([W2[cc, s_, fs[0], g], W2[cc, s_, fs[1], g]], axis=1)
+        return jnp.dot(MIX[g], rhs, preferred_element_type=F32)
+
     def unit(u, cc, s_, fs):
-        rhs = []
-        for g in range(2):
-            rhs.append(jnp.concatenate([W2[cc, s_, fs[0], g], W2[cc, s_, fs[1], g]], axis=1))
-        o = jnp.dot(MIX[0], rhs[0], preferred_element_type=F32)
-        o += jnp.dot(MIX[1], rhs[1], preferred_element_type=F32)
+        leave(u, product(cc, s_, fs, 0) + product(cc, s_, fs, 1))
+
+    def part_unit(u, cc, s_, fs):
+        ACC[:, (u - 14) * 256 : (u - 13) * 256] = product(cc, s_, fs, 0)
+
+    def last_unit(u, cc, s_, fs):
+        leave(u, ACC[:, (u - 14) * 256 : (u - 13) * 256] + product(cc, s_, fs, 1))
+
+    def leave(u, o):
         ob = o.astype(BF16)
         for e in range(2):
             idx = 2 * u + e
@@ -635,10 +650,12 @@
     pair(0, False, ss_, 0, ss_, 1)
     recv(c2a)
     u0, d0 = half_plane(sd, 0), half_plane(su, 1)
-    d2 = [group(W2.at[0, 0, pl.ds(0, 2)]) for _ in range(2)]
-    for k in range(2):
-        send2(u0.at[k], dev_su, d2[k])
-        send2(d0.at[k], dev_sd, d2[k])
+    d2 = [group(W2.at[0, 0, pl.ds(0, 2)]), group(shard2), group(shard2)]
+    send2(u0.at[0], dev_su, d2[0])
+    send2(d0.at[0], dev_sd, d2[0])
+    for g in range(2):
+        send2(u0.at[1, g], dev_su, d2[1 + g])
+        send2(d0.at[1, g], dev_sd, d2[1 + g])
     sib2_a = group(W2.at[0, 0])
     send2(u0, dev_sib, sib2_a)
     send2(d0, dev_sib, sib2_a)
@@ -655,22 +672,30 @@
     recv(sib2_b)
     pair(2, False, ssd, 1, ssu, 0)
 
-    for k in range(2):
-        recv(d2[k])
-        sib2_c = group(W2.at[0, 0, pl.ds(0, 2)])
-        send2(W2.at[c, s2, k], dev_sib, sib2_c)
-        send2(W2.at[c, s2, 2 + k], dev_sib, sib2_c)
-        far_unit(12 + 2 * k, c, s2, k, unit)
-        recv(sib2_c)
-        far_unit(13 + 2 * k, cs, ss2, k, unit)
-        if k == 0:
-            pair(1, True, sd, 0, su, 1, total)
-            pair(1, False, ssd, 0, ssu, 1, total)
+    recv(d2[0])
+    sib2_c = group(W2.at[0, 0, pl.ds(0, 2)])
+    send2(W2.at[c, s2, 0], dev_sib, sib2_c)
+    send2(W2.at[c, s2, 2], dev_sib, sib2_c)
+    far_unit(12, c, s2, 0, unit)
+    recv(sib2_c)
+    far_unit(13, cs, ss2, 0, unit)
+    pair(1, True, sd, 0, su, 1, total)
+    pair(1, False, ssd, 0, ssu, 1, total)
+
+    sib2_d = [group(shard2), group(shard2)]
+    for g in range(2):
+        recv(d2[1 + g])
+        send2(W2.at[c, s2, 1, g], dev_sib, sib2_d[g])
+        send2(W2.at[c, s2, 3, g], dev_sib, sib2_d[g])
+        far_unit(14, c, s2, 1, (part_unit, last_unit)[g])
+    for g in range(2):
+        recv(sib2_d[g])
+        far_unit(15, cs, ss2, 1, (part_unit, last_unit)[g])
 
     wait(W1, ssem.at[W1_SENT])
     wait(W2, ssem.at[W2_SENT])
     wait(TOK.at[0], ssem.at[TOK_SENT])
-    for k, whole in enumerate((SCALE, SINK, ST3, ST3, ST3)):
+    for k, whole in enumerate((SCALE.at[1], SINK.at[1], ST3, ST3, ST3)):
         wait(whole, ssem.at[OTHER_SENT + k])
     for gi in range(2):
         halo_sent(gi)
@@ -685,17 +710,30 @@
     assert len(groups) == N_GROUPS, len(groups)
 
 
+def hand_over(src, out, held, in_sem, out_sem):
+    rows = 256 // PIECES
+    parts = [pl.ds(k * rows, rows) for k in range(PIECES)]
+    ins = [pltpu.make_async_copy(src.at[r], held.at[r], in_sem.at[k]) for k, r in enumerate(parts)]
+    outs = [pltpu.make_async_copy(held.at[r], out.at[r], out_sem.at[k]) for k, r in enumerate(parts)]
+    for d in ins:
+        d.start()
+    for d, o in zip(ins, outs):
+        d.wait()
+        o.start()
+    for o in outs:
+        o.wait()
+
+
 def local_program(
     tokens, norm_gain, w_pool_in, w_query, w_key, w_value, pool_map, pool_scale,
     q_gain, k_gain, sinks, w_out,
 ):
     any_ = pl.BlockSpec(memory_space=pl.ANY)
-    vmem = pl.BlockSpec(memory_space=pltpu.VMEM)
     dma = pltpu.SemaphoreType.DMA
-    return pl.pallas_call(
+    summed = pl.pallas_call(
         kernel,
         out_shape=jax.ShapeDtypeStruct((256, 4096), BF16),
-        in_specs=[any_] * 7 + [vmem] * 5,
+        in_specs=[any_] * 12,
         out_specs=any_,
         scratch_shapes=[
             pltpu.VMEM((2, 2, 4, 4, 128, 1152), BF16),
@@ -705,8 +743,11 @@
             pltpu.VMEM((1024, 128), BF16),
             pltpu.VMEM((256, 512), BF16),
             pltpu.VMEM((2, 512, 512), BF16),
-            pltpu.VMEM((1, 512), F32),
-            pltpu.VMEM((1, 8), F32),
+            pltpu.VMEM((2, 1, 512), F32),
+            pltpu.VMEM((2, 1, 8), F32),
+            pltpu.VMEM((1, 64), F32),
+            pltpu.VMEM((1, 64), F32),
+            pltpu.VMEM((1, 4096), F32),
             pltpu.VMEM((128, 128), BF16),
             pltpu.VMEM((2, 2, 384, 128), BF16),
             pltpu.VMEM((2, 2, 272, 512), BF16),
@@ -721,7 +762,7 @@
             pltpu.VMEM((32, 256, 128), BF16),
             pltpu.VMEM((2, 128, 128), BF16),
             pltpu.VMEM((2, 16, 512), BF16),
-            dma((8,)),
+            dma((13,)),
             dma((9,)),
             dma((N_GROUPS,)),
             dma(()),
@@ -741,6 +782,14 @@
         pool_scale.reshape(1, 512), sinks.reshape(1, 8), q_gain.reshape(1, 64),
         k_gain.reshape(1, 64), norm_gain.reshape(1, 4096),
     )
+    return pl.pallas_call(
+        hand_over,
+        out_shape=jax.ShapeDtypeStruct((256, 4096), BF16),
+        in_specs=[any_],
+        out_specs=any_,
+        scratch_shapes=[pltpu.VMEM((256, 4096), BF16), dma((PIECES,)), dma((PIECES,))],
+        name="hand_over",
+    )(summed)
 
 
 def solution(mesh):

time: 117 us -> 115 us (0.983)
  local copies, waits for them, and re-layouts: 3.13 us -> 0 us
    unnamed x1 -> x0, local copies, waits for them, and re-layouts: 3.13 us -> none
    pallas_call x0 -> x1, Pallas kernels: none -> 2.39 us  [local_program(): pl.pallas_call(hand_over, out_shape=jax.ShapeDtypeStruct((256, 4096), BF1...]
    pallas_call x1, Pallas kernels: 114 us -> 112 us  [local_program(): pl.pallas_call(kernel, out_shape=jax.ShapeDtypeStruct((256, 4096), BF16),...]
where the time goes in v5:
time: 115 us; the launch traced here: 114 us
  Pallas kernels  114 us (99%)
    pallas_call x1, Pallas kernels, local_program(): pl.pallas_call(kernel, out_shape=jax.ShapeDtypeStruct((256, 4096), BF16),...  112 us
    pallas_call x1, Pallas kernels, local_program(): pl.pallas_call(hand_over, out_shape=jax.ShapeDtypeStruct((256, 4096), BF1...  2.39 us

profile of v5, /device:TPU:1, one launch (start us, length us, event | category | flops | bytes accessed | tf_op | source)
XLA Modules:
  0.0 114.4 jit_solution(10335792572978413000)
XLA Ops:
  0.0 111.8 %mixer.1.src = bf16[256,4096]{1,0:T(8,128)(2,1)} custom-call(bf16[1024,1024]{1,0:T(8,128)(2,1)} %tokens.1, bf16[128,512]{1,0:T(8,128)(2,1)} %wp.1, bf16[128,512]{1,0:T(8,128)(2,1)} %wq.1, bf16[64,128]{1,0:T(8,128)(2,1)} %bitcast.9, bf16[64,128]{1,0:T(8,128)(2,1)} %bitcast.10, bf16[1024,128]{1,0:T(8,128)(2,1)} %wo.1, bf16[512,512]{1,0:T(8,128)(2,1)} %bitcast.8, ...), custom_call_target="tpu_custom_call" | custom-call | tf_op jit(solution)/shard_map/mixer/pallas_call | solution.py:733
  111.9 2.4 %hand_over.1 = bf16[256,4096]{1,0:T(8,128)(2,1)} custom-call(bf16[256,4096]{1,0:T(8,128)(2,1)} %mixer.1.src), custom_call_target="tpu_custom_call" | custom-call | tf_op jit(solution)/shard_map/hand_over/pallas_call | solution.py:785

commit v6 on v5

--- a/solution.py
+++ b/solution.py
@@ -9,7 +9,7 @@
 F32 = jnp.float32
 BF16 = jnp.bfloat16
 EPS = 1e-6
-N_GROUPS = 43
+N_GROUPS = 45
 PIECES = 8
 
 
@@ -213,13 +213,14 @@
         send1(W1.at[g, c, s_], dev_sib, to)
 
     def step_a2(g):
-        to = group(shard2)
-        for dev in (dev_fu, dev_fd):
-            send2(W2.at[c, s, f, g], dev, to)
+        to = group(shard2.at[0]), group(shard2.at[0])
+        for k in range(2):
+            send2(W2.at[c, s, f, g, pl.ds(512 * k, 512)], dev_fu, to[k])
+            send2(W2.at[c, s, f, g, pl.ds(512 - 512 * k, 512)], dev_fd, to[k])
         return to
 
     def step_b2(g, a):
-        recv(a)
+        recv(a[0])
         to = group(shard2.at[0])
         send2(W2.at[c, s, fd, g, pl.ds(0, 512)], dev_fu, to)
         send2(W2.at[c, s, fu, g, pl.ds(512, 512)], dev_fd, to)
@@ -536,7 +537,7 @@
     matmul_slab(0, p)
     d1o = step_d1(1, c1o)
     c2a, c2b = group(W2.at[0, 0]), group(W2.at[0, 0])
-    recv(b2)
+    recv(a2[1], b2)
     c2_send(0)
     x_w2 = group(shard2.at[0])
     send(W2.at[c, s, f, 0], ST2, dev_dx, x_w2, W2_SENT)
@@ -572,9 +573,9 @@
     sib1o_far = group(W1.at[0, 0, 0])
     share1(1, s2, sib1o_far)
     matmul_planes(1, c, (s2,))
+    b2o = step_b2(1, a2o)
     recv(sib1o_far)
     matmul_planes(1, cs, (ss2,))
-    b2o = step_b2(1, a2o)
     post(1)
     halo_send(1)
 
@@ -584,7 +585,7 @@
     recv(f_pm)
     sib_pm = group(ST3)
     send(PM.at[1, half], PM.at[1, half], dev_sib, sib_pm, OTHER_SENT + 4)
-    recv(b2o)
+    recv(a2o[1], b2o)
     c2_send(1)
     sib2_own = group(W2.at[0, 0])
     send2(W2.at[c, s], dev_sib, sib2_own)
@@ -603,12 +604,6 @@
     def unit(u, cc, s_, fs):
         leave(u, product(cc, s_, fs, 0) + product(cc, s_, fs, 1))
 
-    def part_unit(u, cc, s_, fs):
-        ACC[:, (u - 14) * 256 : (u - 13) * 256] = product(cc, s_, fs, 0)
-
-    def last_unit(u, cc, s_, fs):
-        leave(u, ACC[:, (u - 14) * 256 : (u - 13) * 256] + product(cc, s_, fs, 1))
-
     def leave(u, o):
         ob = o.astype(BF16)
         for e in range(2):
@@ -650,7 +645,8 @@
     pair(0, False, ss_, 0, ss_, 1)
     recv(c2a)
     u0, d0 = half_plane(sd, 0), half_plane(su, 1)
-    d2 = [group(W2.at[0, 0, pl.ds(0, 2)]), group(shard2), group(shard2)]
+    last = [group(shard2) for _ in range(4)]
+    d2 = [group(W2.at[0, 0, pl.ds(0, 2)]), last[0], last[1]]
     send2(u0.at[0], dev_su, d2[0])
     send2(d0.at[0], dev_sd, d2[0])
     for g in range(2):
@@ -682,15 +678,28 @@
     pair(1, True, sd, 0, su, 1, total)
     pair(1, False, ssd, 0, ssu, 1, total)
 
-    sib2_d = [group(shard2), group(shard2)]
-    for g in range(2):
-        recv(d2[1 + g])
-        send2(W2.at[c, s2, 1, g], dev_sib, sib2_d[g])
-        send2(W2.at[c, s2, 3, g], dev_sib, sib2_d[g])
-        far_unit(14, c, s2, 1, (part_unit, last_unit)[g])
-    for g in range(2):
-        recv(sib2_d[g])
-        far_unit(15, cs, ss2, 1, (part_unit, last_unit)[g])
+    def last_step(t, carry):
+        g, other = lax.rem(t, 2), lax.div(t, 2)
+        wait(shard2, rsem.at[last[0] + t])
+
+        @pl.when(t < 2)
+        def _():
+            for k in (1, 3):
+                send2(W2.at[c, s2, k, g], dev_sib, last[2] + t)
+
+        cc, s_ = c + other * (cs - c), s2 + other * (ss2 - s2)
+        rhs = jnp.concatenate([W2[cc, s_, k, g] for k in (1, 3)], axis=1)
+        o = jnp.dot(MIX[g], rhs, preferred_element_type=F32)
+        o = jnp.where(g == 0, o, ACC[:, 0:256] + o)
+        ACC[:, 0:256] = o
+
+        @pl.when(g == 1)
+        def _():
+            leave(14 + other, ACC[:, 0:256])
+
+        return carry
+
+    lax.fori_loop(0, 4, last_step, 0)
 
     wait(W1, ssem.at[W1_SENT])
     wait(W2, ssem.at[W2_SENT])

time: 115 us -> 112 us (0.974)
  Pallas kernels: 114 us -> 111 us
    pallas_call x1, Pallas kernels: 112 us -> 109 us  [local_program(): pl.pallas_call(kernel, out_shape=jax.ShapeDtypeStruct((256, 4096), BF16),...]
where the time goes in v6:
time: 112 us; the launch traced here: 111 us
  Pallas kernels  111 us (99%)
    pallas_call x1, Pallas kernels, local_program(): pl.pallas_call(kernel, out_shape=jax.ShapeDtypeStruct((256, 4096), BF16),...  109 us
    pallas_call x1, Pallas kernels, local_program(): pl.pallas_call(hand_over, out_shape=jax.ShapeDtypeStruct((256, 4096), BF1...  2.39 us

profile of v6, /device:TPU:1, one launch (start us, length us, event | category | flops | bytes accessed | tf_op | source)
XLA Modules:
  0.0 111.2 jit_solution(11853618659589736311)
XLA Ops:
  0.0 108.6 %mixer.1.src = bf16[256,4096]{1,0:T(8,128)(2,1)} custom-call(bf16[1024,1024]{1,0:T(8,128)(2,1)} %tokens.1, bf16[128,512]{1,0:T(8,128)(2,1)} %wp.1, bf16[128,512]{1,0:T(8,128)(2,1)} %wq.1, bf16[64,128]{1,0:T(8,128)(2,1)} %bitcast.9, bf16[64,128]{1,0:T(8,128)(2,1)} %bitcast.10, bf16[1024,128]{1,0:T(8,128)(2,1)} %wo.1, bf16[512,512]{1,0:T(8,128)(2,1)} %bitcast.8, ...), custom_call_target="tpu_custom_call" | custom-call | tf_op jit(solution)/shard_map/mixer/pallas_call | solution.py:742
  108.6 2.4 %hand_over.1 = bf16[256,4096]{1,0:T(8,128)(2,1)} custom-call(bf16[256,4096]{1,0:T(8,128)(2,1)} %mixer.1.src), custom_call_target="tpu_custom_call" | custom-call | tf_op jit(solution)/shard_map/hand_over/pallas_call | solution.py:794

commit v7 on v6

--- a/solution.py
+++ b/solution.py
@@ -109,8 +109,6 @@
     def greet(dev):
         pl.semaphore_signal(barrier, inc=1, device_id=dev, device_id_type=MESH)
 
-    for dev in (dev_fu, dev_fd, dev_su, dev_sd, dev_sib, dev_p, dev_n, dev_x2):
-        greet(dev)
     @pl.when(relay)
     def _():
         greet(relay_dev)
@@ -127,6 +125,9 @@
         @pl.when(apart)
         def _():
             greet((spp, xp))
+
+    for dev in (dev_x2, dev_su, dev_sd, dev_fu, dev_fd, dev_p, dev_n, dev_sib):
+        greet(dev)
 
     loc = []
 
@@ -534,13 +535,13 @@
     matmul_slab(0, x, True)
     recv(tp_)
     scale_slab(p)
+    x_w2 = group(shard2.at[0])
+    send(W2.at[c, s, f, 0], ST2, dev_dx, x_w2, W2_SENT)
     matmul_slab(0, p)
     d1o = step_d1(1, c1o)
     c2a, c2b = group(W2.at[0, 0]), group(W2.at[0, 0])
     recv(a2[1], b2)
     c2_send(0)
-    x_w2 = group(shard2.at[0])
-    send(W2.at[c, s, f, 0], ST2, dev_dx, x_w2, W2_SENT)
     l6.wait()
     half = pl.ds(c * 256, 256)
     x_pm = group(ST3)
@@ -551,14 +552,14 @@
     recv(tf)
     scale_slab(x2)
     matmul_slab(0, x2)
+    recv(x_w2)
+    f_w2 = group(shard2.at[0])
+    send(ST2, W2.at[c, s, f, 1], dev_dx, f_w2, W2_SENT)
     post(0)
     halo_send(0)
     recv(c1o[1])
     share1(1, sd, sib1o)
     share1(1, su, sib1o)
-    recv(x_w2)
-    f_w2 = group(shard2.at[0])
-    send(ST2, W2.at[c, s, f, 1], dev_dx, f_w2, W2_SENT)
     matmul_planes(1, c, (s, sd, su), True)
     recv(sib1o)
     recv(f_w2)

time: 112 us -> 112 us (level)
  no operation moved by 1% of the time
where the time goes in v7:
time: 112 us; the launch traced here: 111 us
  Pallas kernels  111 us (99%)
    pallas_call x1, Pallas kernels, local_program(): pl.pallas_call(kernel, out_shape=jax.ShapeDtypeStruct((256, 4096), BF16),...  109 us
    pallas_call x1, Pallas kernels, local_program(): pl.pallas_call(hand_over, out_shape=jax.ShapeDtypeStruct((256, 4096), BF1...  2.39 us

profile of v7, /device:TPU:1, one launch (start us, length us, event | category | flops | bytes accessed | tf_op | source)
XLA Modules:
  0.0 111.4 jit_solution(13443161490035355914)
XLA Ops:
  0.0 108.8 %mixer.1.src = bf16[256,4096]{1,0:T(8,128)(2,1)} custom-call(bf16[1024,1024]{1,0:T(8,128)(2,1)} %tokens.1, bf16[128,512]{1,0:T(8,128)(2,1)} %wp.1, bf16[128,512]{1,0:T(8,128)(2,1)} %wq.1, bf16[64,128]{1,0:T(8,128)(2,1)} %bitcast.9, bf16[64,128]{1,0:T(8,128)(2,1)} %bitcast.10, bf16[1024,128]{1,0:T(8,128)(2,1)} %wo.1, bf16[512,512]{1,0:T(8,128)(2,1)} %bitcast.8, ...), custom_call_target="tpu_custom_call" | custom-call | tf_op jit(solution)/shard_map/mixer/pallas_call | solution.py:743
  108.8 2.4 %hand_over.1 = bf16[256,4096]{1,0:T(8,128)(2,1)} custom-call(bf16[256,4096]{1,0:T(8,128)(2,1)} %mixer.1.src), custom_call_target="tpu_custom_call" | custom-call | tf_op jit(solution)/shard_map/hand_over/pallas_call | solution.py:795

commit v8 on v7

--- a/solution.py
+++ b/solution.py
@@ -676,8 +676,6 @@
     far_unit(12, c, s2, 0, unit)
     recv(sib2_c)
     far_unit(13, cs, ss2, 0, unit)
-    pair(1, True, sd, 0, su, 1, total)
-    pair(1, False, ssd, 0, ssu, 1, total)
 
     def last_step(t, carry):
         g, other = lax.rem(t, 2), lax.div(t, 2)
@@ -701,6 +699,8 @@
         return carry
 
     lax.fori_loop(0, 4, last_step, 0)
+    pair(1, True, sd, 0, su, 1, total)
+    pair(1, False, ssd, 0, ssu, 1, total)
 
     wait(W1, ssem.at[W1_SENT])
     wait(W2, ssem.at[W2_SENT])

time: 112 us -> 112 us (level)
  no operation moved by 1% of the time
where the time goes in v8:
time: 112 us; the launch traced here: 111 us
  Pallas kernels  111 us (99%)
    pallas_call x1, Pallas kernels, local_program(): pl.pallas_call(kernel, out_shape=jax.ShapeDtypeStruct((256, 4096), BF16),...  109 us
    pallas_call x1, Pallas kernels, local_program(): pl.pallas_call(hand_over, out_shape=jax.ShapeDtypeStruct((256, 4096), BF1...  2.39 us

profile of v8, /device:TPU:1, one launch (start us, length us, event | category | flops | bytes accessed | tf_op | source)
XLA Modules:
  0.0 111.4 jit_solution(4651347074195867941)
XLA Ops:
  0.0 108.8 %mixer.1.src = bf16[256,4096]{1,0:T(8,128)(2,1)} custom-call(bf16[1024,1024]{1,0:T(8,128)(2,1)} %tokens.1, bf16[128,512]{1,0:T(8,128)(2,1)} %wp.1, bf16[128,512]{1,0:T(8,128)(2,1)} %wq.1, bf16[64,128]{1,0:T(8,128)(2,1)} %bitcast.9, bf16[64,128]{1,0:T(8,128)(2,1)} %bitcast.10, bf16[1024,128]{1,0:T(8,128)(2,1)} %wo.1, bf16[512,512]{1,0:T(8,128)(2,1)} %bitcast.8, ...), custom_call_target="tpu_custom_call" | custom-call | tf_op jit(solution)/shard_map/mixer/pallas_call | solution.py:743
  108.8 2.4 %hand_over.1 = bf16[256,4096]{1,0:T(8,128)(2,1)} custom-call(bf16[256,4096]{1,0:T(8,128)(2,1)} %mixer.1.src), custom_call_target="tpu_custom_call" | custom-call | tf_op jit(solution)/shard_map/hand_over/pallas_call | solution.py:795
